TPU v7x, 32 devices: a whole 2x2x4 slice. The times are simulated.
32 devices in a mesh: ep: 8 (over z, y), tp: 4 (over x, core).
Axes of the slice: x: 2, y: 2, z: 4, core: 2. Of those that a mesh axis runs over, the one named last changes fastest.
Arguments:
- tokens: bfloat16 [192, 1024], P('ep'), may hold values from -6 to 6
- mixer_gain: float32 [1024], replicated, may hold values from 0.1 to 1.9
- gate_weight: bfloat16 [1024, 1024], P(None, 'tp'), may hold values from -0.1875 to 0.1875
- inner_weight: bfloat16 [1024, 1024], P(None, 'tp'), may hold values from -0.1875 to 0.1875
- state_weight: bfloat16 [2, 1024, 512], P(None, None, 'tp'), may hold values from -0.1875 to 0.1875
- step_weight: bfloat16 [1024, 16], P(None, 'tp'), may hold values from -0.1875 to 0.1875
- step_bias: float32 [16], P('tp'), may hold values from -4 to 0.5
- decay_log: float32 [16], P('tp'), may hold values from 0 to 2.8
- skip_scale: float32 [16], P('tp'), may hold values from 0.5 to 1.5
- inner_kernel: float32 [4, 1024], P(None, 'tp'), may hold values from -3 to 3
- state_kernel: float32 [4, 2, 512], P(None, None, 'tp'), may hold values from -3 to 3
- inner_window: bfloat16 [192, 3, 1024], P('ep', None, 'tp'), may hold values from -6 to 6
- state_window: bfloat16 [192, 3, 2, 512], P('ep', None, None, 'tp'), may hold values from -6 to 6
- recurrent_state: float32 [192, 16, 64, 128], P('ep', 'tp'), may hold values from -2.4 to 2.4
- group_gain: float32 [1024], P('tp'), may hold values from 0.1 to 1.9
- output_weight: bfloat16 [1024, 1024], P('tp'), may hold values from -0.1875 to 0.1875
- channel_gain: float32 [1024], replicated, may hold values from 0.1 to 1.9
- routes: int32 [192, 2], P('ep'), may hold values from 0 to 7, all different within a row; in each aligned block of 24 rows (0 to 23, 24 to 47, ...) at most 9 rows name the same one
- route_weights: float32 [192, 2], P('ep'), may hold values from 0.2 to 1
- expert_gate: bfloat16 [8, 1024, 2816], P('ep', None, 'tp'), may hold values from -0.1875 to 0.1875
- expert_up: bfloat16 [8, 1024, 2816], P('ep', None, 'tp'), may hold values from -0.1875 to 0.1875
- expert_down: bfloat16 [8, 2816, 1024], P('ep', 'tp'), may hold values from -0.109375 to 0.109375
- dense_gate: bfloat16 [1024, 2816], P('tp', 'ep'), may hold values from -0.1875 to 0.1875
- dense_up: bfloat16 [1024, 2816], P('tp', 'ep'), may hold values from -0.1875 to 0.1875
- dense_down: bfloat16 [2816, 1024], P('ep', 'tp'), may hold values from -0.109375 to 0.109375
- dense_scale: float32 [1024], P('tp'), may hold values from 0.3 to 1.5
Outputs:
- new_tokens: bfloat16 [192, 1024], P('ep', 'tp')
- new_state: float32 [192, 16, 64, 128], P('ep', 'tp')
- new_inner_window: bfloat16 [192, 3, 1024], P('ep', None, 'tp')
- new_state_window: bfloat16 [192, 3, 2, 512], P('ep', None, None, 'tp')
Inputs may be any that keep to these rules, and one draw needn't show every extreme that they name: `routes`: each row names 2 different experts. Within the rows of one device (aligned blocks of 24 rows) no expert is named by more than 9 rows, and in some block an expert is named by exactly 9 rows.
All inputs are finite; a program needn't handle non-finite values.
Results may differ from a plain program's by a relative error of at most 0.014.
Values may be sent and summed in bfloat16 or wider, within the bound.
A program may use at most 64 MiB of HBM per device.

v0:
```python
import functools

import jax
import jax.numpy as jnp
from jax import lax
from jax.experimental import pallas as pl
from jax.experimental.pallas import tpu as pltpu
from jax.sharding import PartitionSpec as P

HEADS = 16
GROUPS = 4
HEAD_DIM = 64
STATE_DIM = 128


eps = 1e-06


def rms_scale(values, norm_gain):
    squares = jnp.mean(values * values, axis=-1, keepdims=True)
    return values * lax.rsqrt(squares + eps) * norm_gain


def silu(v):
    return v / (1.0 + jnp.exp(-v))


def dot_rows(rows, columns):
    return lax.dot_general(
        rows, columns, (((1,), (1,)), ((), ())), preferred_element_type=jnp.float32
    )


def branches(
    ep_size,
    tp_size,
    part,
    tokens,
    gain,
    mix,
    scale,
    gate_hbm,
    up_hbm,
    down_hbm,
    dgate_hbm,
    dup_hbm,
    ddown_hbm,
    out,
    gate_w,
    up_w,
    down_w,
    dgate_w,
    dup_w,
    ddown_w,
    parts,
    mixes,
    residual,
    rows,
    flat,
    packed,
    pre_send,
    pre_recv,
    hidden,
    y_send,
    y_recv,
    z_send,
    z_recv,
    load_sem,
    part_sems,
    mix_sems,
    row_sems,
    relay_sems,
    pre_sems,
    hid_sems,
    y_sems,
    z_sems,
):
    f32 = jnp.float32
    bf16 = jnp.bfloat16
    me_e = lax.axis_index("ep")
    me_t = lax.axis_index("tp")
    half = lax.rem(me_t, 2)
    partner = me_t + 1 - 2 * half
    count, width = part.shape
    half_width = width // 2
    own_width = width // tp_size
    total = ep_size * count
    block = total // tp_size

    def remote(src, dst, sems, slot, to_e, to_t):
        return pltpu.make_async_remote_copy(
            src_ref=src,
            dst_ref=dst,
            send_sem=sems.at[0, slot],
            recv_sem=sems.at[1, slot],
            device_id=(to_e, to_t),
            device_id_type=pl.DeviceIdType.MESH,
        )

    barrier = pltpu.get_barrier_semaphore()
    for d in range(1, ep_size):
        pl.semaphore_signal(
            barrier,
            inc=1,
            device_id=(lax.rem(me_e + d, ep_size), me_t),
            device_id_type=pl.DeviceIdType.MESH,
        )
    for d in range(1, tp_size):
        pl.semaphore_signal(
            barrier,
            inc=1,
            device_id=(me_e, lax.rem(me_t + d, tp_size)),
            device_id_type=pl.DeviceIdType.MESH,
        )
    loads = []
    for i, (src, dst) in enumerate(
        [
            (dgate_hbm, dgate_w),
            (dup_hbm, dup_w),
            (gate_hbm, gate_w),
            (up_hbm, up_w),
            (down_hbm, down_w),
            (ddown_hbm, ddown_w),
        ]
    ):
        copy = pltpu.make_async_copy(src, dst, load_sem.at[i])
        copy.start()
        loads.append(copy)
    pl.semaphore_wait(barrier, ep_size + tp_size - 2)

    ep_peers = [lax.rem(me_e + d, ep_size) for d in range(ep_size)]
    tp_peers = [lax.rem(me_t + d, tp_size) for d in range(tp_size)]
    part_copies = [
        remote(part, parts.at[d], part_sems, d, me_e, tp_peers[d]) for d in range(1, tp_size)
    ]
    for copy in part_copies:
        copy.start()
    mix_copies = [
        remote(mix, mixes.at[d], mix_sems, d, ep_peers[d], me_t) for d in range(1, ep_size)
    ]
    for copy in mix_copies:
        copy.start()

    value = tokens[...].astype(f32) + part[...].astype(f32)
    for d in range(1, tp_size):
        part_copies[d - 1].wait_recv()
        value = value + parts[d].astype(f32)
    residual[...] = value
    ffn = rms_scale(value, gain[...]).astype(bf16)
    rows[0, 0] = ffn[:, :half_width]
    rows[1, 0] = ffn[:, half_width:]
    row_copies = [
        remote(rows.at[half, 0], rows.at[half, d], row_sems, d, ep_peers[d], me_t)
        for d in range(1, ep_size)
    ]
    for copy in row_copies:
        copy.start()
    relay_copies = []
    for d in range(1, ep_size):
        row_copies[d - 1].wait_recv()
        copy = remote(rows.at[half, d], rows.at[half, d], relay_sems, d, me_e, partner)
        copy.start()
        relay_copies.append(copy)
    for copy in relay_copies:
        copy.wait_recv()
    for d in range(ep_size):
        flat[d * count : (d + 1) * count, :half_width] = rows[0, d].astype(f32)
        flat[d * count : (d + 1) * count, half_width:] = rows[1, d].astype(f32)
    packed[...] = flat[...].astype(bf16)

    loads[0].wait()
    loads[1].wait()
    own = pl.ds(pl.multiple_of(me_t * own_width, own_width), own_width)
    for t in range(tp_size):
        piece = packed[t * block : (t + 1) * block, own]
        pre_send[t, 0] = dot_rows(piece, dgate_w[...]).astype(bf16)
        pre_send[t, 1] = dot_rows(piece, dup_w[...]).astype(bf16)
    pre_copies = [
        remote(pre_send.at[tp_peers[d]], pre_recv.at[d], pre_sems, d, me_e, tp_peers[d])
        for d in range(1, tp_size)
    ]
    for copy in pre_copies:
        copy.start()

    for d in range(1, ep_size):
        mix_copies[d - 1].wait_recv()
    mixes[0] = mix[...]
    loads[2].wait()
    loads[3].wait()
    loads[4].wait()

    chunk_blocks = 8 if ep_size % 8 == 0 else 1
    chunk = chunk_blocks * count

    def experts(step, carry):
        at = pl.ds(pl.multiple_of(step * chunk, chunk), chunk)
        x = packed[at, :]
        gate_act = dot_rows(x, gate_w[0])
        up_act = dot_rows(x, up_w[0])
        activated = (silu(gate_act) * up_act).astype(bf16)
        weights = mixes[pl.ds(step * chunk_blocks, chunk_blocks)].reshape(chunk, mix.shape[1])
        lanes = lax.broadcasted_iota(jnp.int32, weights.shape, 1)
        weight = jnp.sum(jnp.where(lanes == me_e, weights, 0.0), axis=1, keepdims=True)
        for t in range(tp_size):
            y = jnp.dot(
                activated,
                down_w[0, :, t * own_width : (t + 1) * own_width],
                preferred_element_type=f32,
            )
            y_send[t, at, :] = (y * weight).astype(bf16)
        return carry

    lax.fori_loop(0, total // chunk, experts, 0)
    y_copies = [
        remote(y_send.at[tp_peers[d]], y_recv.at[d], y_sems, d, me_e, tp_peers[d])
        for d in range(1, tp_size)
    ]

    gate_sum = pre_send[me_t, 0].astype(f32)
    up_sum = pre_send[me_t, 1].astype(f32)
    for d in range(1, tp_size):
        pre_copies[d - 1].wait_recv()
        gate_sum = gate_sum + pre_recv[d, 0].astype(f32)
        up_sum = up_sum + pre_recv[d, 1].astype(f32)
    hidden[me_t] = (silu(gate_sum) * up_sum).astype(bf16)
    hid_copies = [
        remote(hidden.at[me_t], hidden.at[me_t], hid_sems, d, me_e, tp_peers[d])
        for d in range(1, tp_size)
    ]
    for copy in hid_copies:
        copy.start()
    for copy in y_copies:
        copy.start()
    for d in range(1, tp_size):
        hid_copies[d - 1].wait_recv()
    loads[5].wait()
    for t in range(tp_size):
        dense = jnp.dot(hidden[t], ddown_w[...], preferred_element_type=f32) * scale[...]
        flat[t * block : (t + 1) * block, :own_width] = dense
    for d in range(1, tp_size):
        y_copies[d - 1].wait_recv()

    def combine(step, carry):
        at = pl.ds(pl.multiple_of(step * chunk, chunk), chunk)
        summed = flat[at, :own_width] + y_send[me_t, at, :].astype(f32)
        for d in range(1, tp_size):
            summed = summed + y_recv[d, at, :].astype(f32)
        for i in range(chunk_blocks):
            z_send[step * chunk_blocks + i] = summed[i * count : (i + 1) * count].astype(bf16)
        return carry

    lax.fori_loop(0, total // chunk, combine, 0)
    z_copies = [
        remote(
            z_send.at[d],
            z_recv.at[d],
            z_sems,
            d,
            lax.rem(me_e + ep_size - d, ep_size),
            me_t,
        )
        for d in range(1, ep_size)
    ]
    for copy in z_copies:
        copy.start()
    final = residual[:, own] + z_send[0].astype(f32)
    for d in range(1, ep_size):
        z_copies[d - 1].wait_recv()
        final = final + z_recv[d].astype(f32)
    out[...] = final.astype(bf16)
    for copy in part_copies + mix_copies + row_copies + relay_copies + pre_copies:
        copy.wait_send()
    for copy in hid_copies + y_copies + z_copies:
        copy.wait_send()


def local(
    tokens,
    mixer_gain,
    gate_weight,
    inner_weight,
    state_weight,
    step_weight,
    step_bias,
    decay_log,
    skip_scale,
    inner_kernel,
    state_kernel,
    inner_window,
    state_window,
    recurrent_state,
    group_gain,
    output_weight,
    channel_gain,
    routes,
    route_weights,
    expert_gate,
    expert_up,
    expert_down,
    dense_gate,
    dense_up,
    dense_down,
    dense_scale,
):
    f32 = jnp.float32
    bf16 = jnp.bfloat16
    seq_count = tokens.shape[0]
    residual = tokens.astype(f32)
    normed = rms_scale(residual, mixer_gain).astype(bf16)
    gate_pre = jnp.dot(normed, gate_weight, preferred_element_type=f32)
    inner_pre = jnp.dot(normed, inner_weight, preferred_element_type=f32).astype(bf16)
    state_pre = jnp.stack(
        [
            jnp.dot(normed, state_weight[0], preferred_element_type=f32),
            jnp.dot(normed, state_weight[1], preferred_element_type=f32),
        ],
        axis=1,
    ).astype(bf16)
    step_raw = jnp.dot(normed, step_weight, preferred_element_type=f32)
    inner_ctx = jnp.concatenate([inner_window, inner_pre[:, None, :]], axis=1)
    inner_conv = jax.nn.silu(jnp.sum(inner_ctx.astype(f32) * inner_kernel[None], axis=1))
    state_ctx = jnp.concatenate([state_window, state_pre[:, None]], axis=1)
    state_conv = jax.nn.silu(jnp.sum(state_ctx.astype(f32) * state_kernel[None], axis=1))
    per_group = HEADS // GROUPS
    local_groups = state_conv.shape[-1] // STATE_DIM
    step_size = jax.nn.softplus(step_raw + step_bias)
    decay_rate = jnp.exp(-step_size * jnp.exp(decay_log))
    shaped = (seq_count, local_groups, per_group)
    inner_heads = inner_conv.reshape(seq_count, local_groups, per_group, HEAD_DIM)
    in_vector = state_conv[:, 0].reshape(seq_count, local_groups, STATE_DIM)
    out_vector = state_conv[:, 1].reshape(seq_count, local_groups, STATE_DIM)
    old_state = recurrent_state.reshape(seq_count, local_groups, per_group, HEAD_DIM, STATE_DIM)
    written = (step_size.reshape(shaped)[..., None] * inner_heads)[..., None] * in_vector[
        :, :, None, None, :
    ]
    new_state = old_state * decay_rate.reshape(shaped)[..., None, None] + written
    mixed_out = jnp.sum(new_state * out_vector[:, :, None, None, :], axis=-1)
    mixed_out = (
        mixed_out + skip_scale.reshape(local_groups, per_group)[None, :, :, None] * inner_heads
    )
    gated_out = mixed_out.reshape(seq_count, -1) * jax.nn.silu(gate_pre)
    grouped = rms_scale(gated_out.reshape(seq_count, local_groups, -1), 1.0).reshape(seq_count, -1)
    mixer_rows = (grouped * group_gain).astype(bf16)
    partial_value = jnp.dot(mixer_rows, output_weight, preferred_element_type=f32).astype(bf16)
    ep_size = lax.axis_size("ep")
    tp_size = lax.axis_size("tp")
    width = tokens.shape[1]
    own_width = width // tp_size
    total = ep_size * seq_count
    block = total // tp_size
    hidden_width = dense_gate.shape[1]
    expert_gate = jnp.swapaxes(expert_gate, 1, 2)
    expert_up = jnp.swapaxes(expert_up, 1, 2)
    dense_gate = dense_gate.T
    dense_up = dense_up.T
    lanes = -(-ep_size // 128) * 128
    mix = jnp.sum(
        jnp.where(
            routes[:, :, None] == jnp.arange(lanes, dtype=jnp.int32)[None, None, :],
            route_weights[:, :, None],
            0.0,
        ),
        axis=1,
    )
    vmem = pl.BlockSpec(memory_space=pltpu.VMEM)
    hbm = pl.BlockSpec(memory_space=pl.ANY)
    dma = pltpu.SemaphoreType.DMA
    new_tokens = pl.pallas_call(
        functools.partial(branches, ep_size, tp_size),
        out_shape=jax.ShapeDtypeStruct((seq_count, own_width), bf16),
        in_specs=[vmem] * 5 + [hbm] * 6,
        out_specs=vmem,
        scratch_shapes=[
            pltpu.VMEM(expert_gate.shape, bf16),
            pltpu.VMEM(expert_up.shape, bf16),
            pltpu.VMEM(expert_down.shape, bf16),
            pltpu.VMEM(dense_gate.shape, bf16),
            pltpu.VMEM(dense_up.shape, bf16),
            pltpu.VMEM(dense_down.shape, bf16),
            pltpu.VMEM((tp_size, seq_count, width), bf16),
            pltpu.VMEM((ep_size, seq_count, lanes), f32),
            pltpu.VMEM((seq_count, width), f32),
            pltpu.VMEM((2, ep_size, seq_count, width // 2), bf16),
            pltpu.VMEM((total, width), f32),
            pltpu.VMEM((total, width), bf16),
            pltpu.VMEM((tp_size, 2, block, hidden_width), bf16),
            pltpu.VMEM((tp_size, 2, block, hidden_width), bf16),
            pltpu.VMEM((tp_size, block, hidden_width), bf16),
            pltpu.VMEM((tp_size, total, own_width), bf16),
            pltpu.VMEM((tp_size, total, own_width), bf16),
            pltpu.VMEM((ep_size, seq_count, own_width), bf16),
            pltpu.VMEM((ep_size, seq_count, own_width), bf16),
            dma((6,)),
            dma((2, tp_size)),
            dma((2, ep_size)),
            dma((2, ep_size)),
            dma((2, ep_size)),
            dma((2, tp_size)),
            dma((2, tp_size)),
            dma((2, tp_size)),
            dma((2, ep_size)),
        ],
        compiler_params=pltpu.CompilerParams(
            collective_id=0, has_side_effects=True, vmem_limit_bytes=60 * 1024 * 1024
        ),
    )(
        partial_value,
        tokens,
        channel_gain[None],
        mix,
        dense_scale[None],
        expert_gate,
        expert_up,
        expert_down,
        dense_gate,
        dense_up,
        dense_down,
    )
    return (
        new_tokens,
        new_state.reshape(seq_count, -1, HEAD_DIM, STATE_DIM),
        inner_ctx[:, 1:],
        state_ctx[:, 1:],
    )


def solution(mesh):
    placed = (
        P("ep", None),
        P(),
        P(None, "tp"),
        P(None, "tp"),
        P(None, None, "tp"),
        P(None, "tp"),
        P("tp"),
        P("tp"),
        P("tp"),
        P(None, "tp"),
        P(None, None, "tp"),
        P("ep", None, "tp"),
        P("ep", None, None, "tp"),
        P("ep", "tp", None, None),
        P("tp"),
        P("tp", None),
        P(),
        P("ep", None),
        P("ep", None),
        P("ep", None, "tp"),
        P("ep", None, "tp"),
        P("ep", "tp", None),
        P("tp", "ep"),
        P("tp", "ep"),
        P("ep", "tp"),
        P("tp"),
    )
    return jax.shard_map(
        local,
        mesh=mesh,
        in_specs=placed,
        out_specs=(
            P("ep", "tp"),
            P("ep", "tp", None, None),
            P("ep", None, "tp"),
            P("ep", None, None, "tp"),
        ),
        check_vma=False,
    )
```

profile of v0, /device:TPU:0, one launch (start us, length us, event | category | flops | bytes accessed | tf_op | source)
XLA Modules:
  0.0 54.7 jit_solution(4496111890614216864)
XLA Ops:
  0.6 0.0 copy-start
  0.6 1.0 %fusion.7 = f32[24]{0:T(128)S(1)} fusion(bf16[24,1024]{1,0:T(8,128)(2,1)} %tokens.1), kind=kLoop, calls=%fused_computation.16 | loop fusion | flops 73704 | bytes 49248 | tf_op jit(solution)/shard_map/reduce_sum | solution.py:20
  1.6 1.3 %fusion = bf16[24,1,256]{2,0,1:T(8,128)(2,1)S(1)} fusion(bf16[1024,256]{1,0:T(8,128)(2,1)} %param.29, bf16[24,1024]{1,0:T(8,128)(2,1)} %tokens.1, f32[1024]{0:T(1024)} %param.27, f32[24]{0:T(128)S(1)} %add_rsqrt_fusion.1), kind=kOutput, calls=%fused_computation.4 | convolution fusion | flops 12687360 | bytes 589920 | tf_op jit(solution)/shard_map/dot_general | solution.py:311
  2.9 0.8 %multiply_reduce_fusion.2 = f32[24,256]{1,0:T(8,128)S(1)} fusion(bf16[24,1,256]{2,0,1:T(8,128)(2,1)S(1)} %fusion, bf16[24,3,256]{2,0,1:T(8,128)(2,1)} %param.37, f32[4,256]{1,0:T(4,128)} %param.35), kind=kLoop, calls=%fused_computation.20 | loop fusion | flops 92160 | bytes 77824 | tf_op jit(solution)/shard_map/reduce_sum | solution.py:321
  3.7 0.1 reduce_sum.60
  3.8 0.7 %exp.33 = f32[4]{0:T(128)S(1)} exponential(f32[4]{0:T(128)} %param.33) | non-fusion elementwise | bytes 32 | tf_op jit(solution)/shard_map/exp | solution.py:327
  4.5 1.0 %multiply_exponential_fusion = (f32[24,4]{0,1:T(4,128)S(1)}, f32[24,4]{0,1:T(4,128)S(1)}) fusion(f32[4]{0:T(128)S(1)} %exp.33, f32[4]{0:T(128)} %param.32, bf16[1024,4]{0,1:T(4,128)(2,1)} %param.31, bf16[24,1024]{1,0:T(8,128)(2,1)} %tokens.1, f32[1024]{0:T(1024)} %param.27, f32[24]{0:T(128)S(1)} %add_rsqrt_fusion.1), kind=kOutput, calls=%fused_computation.39 | convolution fusion | flops 295776 | bytes 62336 | tf_op jit(solution)/shard_map/dot_general | solution.py:319
  5.5 0.1 copy.41
  5.6 0.1 fusion.10
  5.7 1.2 %fusion.1 = bf16[24,1,1,128]{3,0,2,1:T(8,128)(2,1)S(1)} fusion(bf16[2,1024,128]{2,1,0:T(8,128)(2,1)} %param.30, bf16[24,1024]{1,0:T(8,128)(2,1)} %tokens.1, f32[1024]{0:T(1024)} %param.27, f32[24]{0:T(128)S(1)} %add_rsqrt_fusion.1), kind=kOutput, calls=%fused_computation.7 | convolution fusion | flops 6392832 | bytes 321632 | tf_op jit(solution)/shard_map/dot_general | solution.py:314
  6.9 1.2 %fusion.2 = bf16[24,1,1,128]{3,0,2,1:T(8,128)(2,1)S(1)} fusion(bf16[2,1024,128]{2,1,0:T(8,128)(2,1)} %param.30, bf16[24,1024]{1,0:T(8,128)(2,1)} %tokens.1, f32[1024]{0:T(1024)} %param.27, f32[24]{0:T(128)S(1)} %add_rsqrt_fusion.1), kind=kOutput, calls=%fused_computation.8 | convolution fusion | flops 6392832 | bytes 321632 | tf_op jit(solution)/shard_map/dot_general | solution.py:315
  8.2 0.8 %constant_dynamic-update-slice_fusion = bf16[24,4,2,128]{3,2,1,0:T(2,128)(2,1)S(1)} fusion(bf16[24,3,2,128]{3,2,1,0:T(2,128)(2,1)} %param.38), kind=kLoop, calls=%fused_computation.37 | loop fusion | bytes 73728
  9.0 0.8 %multiply_reduce_fusion.1 = f32[24,2,128]{2,1,0:T(2,128)S(1)} fusion(bf16[24,4,2,128]{3,2,1,0:T(2,128)(2,1)S(1)} %copy_dynamic-update-slice_fusion, f32[4,2,128]{2,1,0:T(2,128)} %param.36), kind=kLoop, calls=%fused_computation.19 | loop fusion | flops 67584 | bytes 77824 | tf_op jit(solution)/shard_map/reduce_sum | solution.py:323
  9.8 0.1 copy.40
  9.9 0.0 copy-start.5
  9.9 0.0 copy-start.6
  10.0 0.0 copy-start.7
  10.0 4.4 %multiply_reduce_fusion = (f32[24,4,64]{2,1,0:T(4,128)S(1)}, f32[24,4,64,128]{3,2,1,0:T(8,128)}) fusion(f32[24,128]{1,0:T(8,128)S(1)} %bitcast.29, f32[24,128]{1,0:T(8,128)S(1)} %bitcast.28, f32[24,4,64]{2,1,0:T(4,128)S(1)} %fusion.10, f32[24,4,64,128]{3,2,1,0:T(8,128)} %param.39, f32[24,4]{1,0:T(8,128)S(1)} %copy.40), kind=kLoop, calls=%fused_computation | loop fusion | flops 3926016 | bytes 6365568 | tf_op jit(solution)/shard_map/reduce_sum | solution.py:337
  14.3 0.1 reduce_sum.63
  14.4 0.0 copy-done.8
  14.4 0.1 mul.178
  14.5 0.1 mul.179
  14.6 0.0 copy-done.1
  14.6 0.0 copy-done.2
  14.6 0.0 copy-start.3
  14.6 0.4 multiply_reduce_fusion.3
  15.0 0.8 %convolution_convert_fusion.part = bf16[24,1024]{1,0:T(8,128)(2,1)} fusion(bf16[256,1024]{1,0:T(8,128)(2,1)S(1)} %copy-done, f32[24,256]{1,0:T(8,128)S(1)} %get-tuple-element.11, f32[256]{0:T(256)S(1)} %copy-done.5, f32[24]{0:T(128)S(1)} %add_rsqrt_fusion), kind=kOutput, calls=%fused_computation.2 | convolution fusion | flops 12625920 | bytes 599136 | tf_op jit(solution)/shard_map/dot_general | solution.py:344
  15.8 0.7 %select_reduce_fusion.mix = f32[24,128]{1,0:T(8,128)} fusion(f32[24,2]{0,1:T(2,128)S(1)} %copy-done.6, s32[24,2]{0,1:T(2,128)S(1)} %copy-done.7), kind=kLoop, calls=%fused_computation.28 | loop fusion | flops 15360 | bytes 12672 | tf_op jit(solution)/shard_map/reduce_sum | solution.py:357
  16.5 35.6 %shard_map.273 = bf16[24,256]{1,0:T(8,128)(2,1)} custom-call(bf16[24,1024]{1,0:T(8,128)(2,1)} %convolution_convert_fusion.part, bf16[24,1024]{1,0:T(8,128)(2,1)} %tokens.1, f32[1,1024]{1,0:T(1,128)} %bitcast.30, f32[24,128]{1,0:T(8,128)} %select_reduce_fusion.mix, f32[1,256]{1,0:T(1,128)} %bitcast.31, bf16[1,704,1024]{2,1,0:T(8,128)(2,1)} %bitcast.24, ...), custom_call_target="tpu_custom_call" | custom-call | tf_op jit(solution)/shard_map/pallas_call | solution.py:368
  52.2 0.6 %slice.28 = bf16[24,3,2,128]{3,2,1,0:T(2,128)(2,1)} slice(bf16[24,4,2,128]{3,2,1,0:T(2,128)(2,1)S(1)} %copy_dynamic-update-slice_fusion), slice={[0:24], [1:4], [0:2], [0:128]} | slice | bytes 73728 | tf_op jit(solution)/shard_map/slice | solution.py:423
  52.8 0.6 %fusion.11 = bf16[24,3,256]{2,0,1:T(8,128)(2,1)} fusion(bf16[24,3,256]{2,0,1:T(8,128)(2,1)S(1)} %copy-done.3, bf16[24,1,256]{2,0,1:T(8,128)(2,1)S(1)} %fusion), kind=kLoop, calls=%fused_computation.26 | loop fusion | flops 18432 | bytes 86016 | tf_op jit(solution)/shard_map/concatenate | solution.py:320
  53.4 1.3 %copy.46 = bf16[24,256]{1,0:T(8,128)(2,1)} copy(bf16[24,256]{1,0:T(8,128)(2,1)} %shard_map.273) | data formatting | bytes 24576
  (16 shorter events, 0.1 us)
Async XLA Ops:
  0.6 14.3 %copy-start = (bf16[256,1024]{1,0:T(8,128)(2,1)S(1)}, bf16[256,1024]{1,0:T(8,128)(2,1)}, u32[]{:S(2)}) copy-start(bf16[256,1024]{1,0:T(8,128)(2,1)} %param.41) | copy-start | bytes 1572868
  9.9 4.5 %copy-start.8 = (f32[4]{0:T(128)S(1)}, f32[4]{0:T(128)}, u32[]{:S(2)}) copy-start(f32[4]{0:T(128)} %param.34) | copy-start | bytes 52
  9.9 4.7 %copy-start.1 = (bf16[24,1024]{1,0:T(8,128)(2,1)S(1)}, bf16[24,1024]{1,0:T(8,128)(2,1)}, u32[]{:S(2)}) copy-start(bf16[24,1024]{1,0:T(8,128)(2,1)} %tokens.1) | copy-start | bytes 147460
  9.9 4.7 %copy-start.2 = (bf16[1024,256]{1,0:T(8,128)(2,1)S(1)}, bf16[1024,256]{1,0:T(8,128)(2,1)}, u32[]{:S(2)}) copy-start(bf16[1024,256]{1,0:T(8,128)(2,1)} %param.28) | copy-start | bytes 1572868
  9.9 4.7 %copy-start.4 = (f32[1024]{0:T(1024)S(1)}, f32[1024]{0:T(1024)}, u32[]{:S(2)}) copy-start(f32[1024]{0:T(1024)} %param.27) | copy-start | bytes 12292
  9.9 5.0 %copy-start.5 = (f32[256]{0:T(256)S(1)}, f32[256]{0:T(256)}, u32[]{:S(2)}) copy-start(f32[256]{0:T(256)} %param.40) | copy-start | bytes 3076
  9.9 5.9 %copy-start.6 = (f32[24,2]{0,1:T(2,128)S(1)}, f32[24,2]{0,1:T(2,128)}, u32[]{:S(2)}) copy-start(f32[24,2]{0,1:T(2,128)} %param.44) | copy-start | bytes 580
  10.0 5.9 %copy-start.7 = (s32[24,2]{0,1:T(2,128)S(1)}, s32[24,2]{0,1:T(2,128)}, u32[]{:S(2)}) copy-start(s32[24,2]{0,1:T(2,128)} %param.43) | copy-start | bytes 580
  14.6 38.2 %copy-start.3 = (bf16[24,3,256]{2,0,1:T(8,128)(2,1)S(1)}, bf16[24,3,256]{2,0,1:T(8,128)(2,1)}, u32[]{:S(2)}) copy-start(bf16[24,3,256]{2,0,1:T(8,128)(2,1)} %param.37) | copy-start | bytes 110596
where the time goes:
time: 55.8 us; the launch traced here: 54.7 us
  Pallas kernels  35.6 us (64%)
  other arithmetic  8.35 us (15%)
  matrix products  5.97 us (11%)
  local copies, waits for them, and re-layouts  4.01 us (7%)
  between operations  0.78 us (1%)
    pallas_call x1, Pallas kernels, local(): pl.pallas_call(functools.partial(branches, ep_size, tp_size), out_shape=j...  35.6 us
    reduce_sum x1, other arithmetic, local(): mixed_out = jnp.sum(new_state * out_vector[:, :, None, None, :], axis=-1)  4.36 us
    unnamed x20, local copies, waits for them, and re-layouts  2.15 us
    dot_general x1, matrix products, local(): jnp.dot(normed, inner_weight, preferred_element_type=f32).astype(bf16)  1.32 us
    dot_general x1, matrix products, local(): jnp.dot(normed, state_weight[1], preferred_element_type=f32)  1.21 us
    dot_general x1, matrix products, local(): jnp.dot(normed, state_weight[0], preferred_element_type=f32)  1.2 us

commit v1 on v0

v1 whole, which is shorter than its diff:
```python
import functools

import jax
import jax.numpy as jnp
from jax import lax
from jax.experimental import pallas as pl
from jax.experimental.pallas import tpu as pltpu
from jax.sharding import PartitionSpec as P

HEADS = 16
GROUPS = 4
HEAD_DIM = 64
STATE_DIM = 128
LANES = 128
SEQ_STEP = 4

eps = 1e-06


def silu(v):
    return v / (1.0 + jnp.exp(-v))


def dot_rows(rows, columns):
    return lax.dot_general(
        rows, columns, (((1,), (1,)), ((), ())), preferred_element_type=jnp.float32
    )


def dot(a, b):
    return jnp.dot(a, b, preferred_element_type=jnp.float32)


def mixer(
    tokens_hbm,
    mgain_hbm,
    gatew_hbm,
    innerw_hbm,
    statew_hbm,
    stepw_hbm,
    sbias_hbm,
    dlog_hbm,
    skip_hbm,
    ikern_hbm,
    skern_hbm,
    iwin_hbm,
    swin_hbm,
    state_hbm,
    ggain_hbm,
    rows_out,
    state_out,
    iwin_out,
    swin_out,
    tokens,
    mgain,
    gatew,
    innerw,
    statew,
    stepw,
    sbias,
    dlog,
    skip,
    ikern,
    skern,
    iwin,
    swin,
    state,
    ggain,
    decays,
    mixed,
    rows,
    sems,
    state_sems,
    out_sems,
):
    f32 = jnp.float32
    bf16 = jnp.bfloat16
    count = tokens.shape[0]
    taps = ikern.shape[0]
    heads = sbias.shape[1]
    inner = innerw.shape[1]
    head_dim = inner // heads
    n_state = statew.shape[2]
    small = [
        (tokens_hbm, tokens),
        (mgain_hbm, mgain),
        (innerw_hbm, innerw),
        (statew_hbm, statew),
        (stepw_hbm, stepw),
        (sbias_hbm, sbias),
        (dlog_hbm, dlog),
        (ikern_hbm, ikern),
        (skern_hbm, skern),
        (iwin_hbm, iwin.at[pl.ds(0, taps - 1)]),
        (swin_hbm, swin.at[:, pl.ds(0, taps - 1)]),
        (gatew_hbm, gatew),
        (skip_hbm, skip),
        (ggain_hbm, ggain),
    ]
    loads = []
    for i, (src, dst) in enumerate(small):
        copy = pltpu.make_async_copy(src, dst, sems.at[i])
        copy.start()
        loads.append(copy)

    def state_load(i):
        at = pl.ds(i * SEQ_STEP, SEQ_STEP)
        return pltpu.make_async_copy(state_hbm.at[at], state.at[at], state_sems.at[0, i])

    def state_store(i):
        at = pl.ds(i * SEQ_STEP, SEQ_STEP)
        return pltpu.make_async_copy(state.at[at], state_out.at[at], state_sems.at[1, i])

    steps = count // SEQ_STEP
    for i in range(steps):
        state_load(i).start()

    loads[0].wait()
    loads[1].wait()
    value = tokens[...].astype(f32)
    squares = jnp.mean(value * value, axis=-1, keepdims=True)
    normed = (value * lax.rsqrt(squares + eps) * mgain[...]).astype(bf16)
    for i in range(2, 11):
        loads[i].wait()
    inner_pre = dot(normed, innerw[...]).astype(bf16)
    pre_u = dot(normed, statew[0])
    pre_c = dot(normed, statew[1])
    step_raw = dot_rows(normed, stepw[...])

    iwin[taps - 1] = inner_pre
    conv = inner_pre.astype(f32) * ikern[taps - 1 : taps, :]
    for j in range(taps - 1):
        conv = conv + iwin[j].astype(f32) * ikern[j : j + 1, :]
    inner_conv = silu(conv)

    both = jnp.concatenate([pre_u[:, None, :], pre_c[:, None, :]], axis=1).astype(bf16)
    swin[:, taps - 1] = both
    sconv = both.astype(f32) * skern[taps - 1][None]
    for j in range(taps - 1):
        sconv = sconv + swin[:, j].astype(f32) * skern[j][None]
    sconv = silu(sconv)
    u_vec = sconv[:, 0, :]
    c_vec = sconv[:, 1, :].astype(bf16)
    win_copies = [
        pltpu.make_async_copy(iwin.at[pl.ds(1, taps - 1)], iwin_out, out_sems.at[0]),
        pltpu.make_async_copy(swin.at[:, pl.ds(1, taps - 1)], swin_out, out_sems.at[1]),
    ]
    for copy in win_copies:
        copy.start()

    step_size = jax.nn.softplus(step_raw + sbias[...])
    decay = jnp.exp(-step_size * jnp.exp(dlog[...]))
    step_wide = jnp.concatenate(
        [jnp.broadcast_to(step_size[:, h : h + 1], (count, head_dim)) for h in range(heads)],
        axis=1,
    )
    for h in range(heads):
        decays[:, h * n_state : (h + 1) * n_state] = jnp.broadcast_to(
            decay[:, h : h + 1], (count, n_state)
        )
    written = (step_wide * inner_conv).T.astype(bf16)
    row_of = lax.broadcasted_iota(jnp.int32, (count, n_state), 0)
    mixed_row = lax.broadcasted_iota(jnp.int32, (count, inner), 0)
    mixed[...] = jnp.zeros_like(mixed)

    def update(i, carry):
        state_load(i).wait()
        total = mixed[...]
        for k in range(0, SEQ_STEP, 2):
            b = i * SEQ_STEP + k
            pair = jnp.concatenate(
                [jnp.where(row_of == b + n, u_vec, 0.0) for n in range(2)], axis=1
            ).astype(bf16)
            outer = dot(written, pair)
            for n in range(2):
                fade = decays[pl.ds(b + n, 1), :]
                parts = []
                for h in range(heads):
                    new = state[b + n, h] * fade[:, h * n_state : (h + 1) * n_state]
                    new = new + outer[
                        h * head_dim : (h + 1) * head_dim, n * n_state : (n + 1) * n_state
                    ]
                    state[b + n, h] = new
                    parts.append(new.astype(bf16))
                read = dot_rows(c_vec, jnp.concatenate(parts, axis=0))
                total = jnp.where(mixed_row == b + n, read, total)
        mixed[...] = total
        state_store(i).start()
        return carry

    lax.fori_loop(0, steps, update, 0)
    for i in range(11, 14):
        loads[i].wait()
    gate_pre = dot(normed, gatew[...])
    skip_wide = jnp.concatenate(
        [jnp.broadcast_to(skip[:, h : h + 1], (1, head_dim)) for h in range(heads)], axis=1
    )
    gated = (mixed[...] + skip_wide * inner_conv) * silu(gate_pre)
    squares = jnp.mean(gated * gated, axis=-1, keepdims=True)
    rows[...] = (gated * lax.rsqrt(squares + eps) * ggain[...]).astype(bf16)
    last = pltpu.make_async_copy(rows, rows_out, out_sems.at[2])
    last.start()
    for i in range(steps):
        state_store(i).wait()
    for copy in win_copies:
        copy.wait()
    last.wait()


def flip(index, mask):
    moved = index
    bit = 1
    while bit <= mask:
        if mask & bit:
            moved = moved + bit * (1 - 2 * lax.rem(index // bit, 2))
        bit *= 2
    return moved


def branches(
    ep_size,
    tp_size,
    slice_rows,
    rows_hbm,
    outw_hbm,
    tokens_hbm,
    gain_hbm,
    routes_hbm,
    rweights_hbm,
    scale_hbm,
    gate_hbm,
    up_hbm,
    down_hbm,
    dgate_hbm,
    dup_hbm,
    ddown_hbm,
    out,
    mrows,
    outw,
    tokens,
    gain,
    routes,
    rweights,
    scales,
    gate_w,
    up_w,
    down_w,
    dense_w,
    tables,
    part,
    parts,
    residual,
    rows,
    flat,
    packed,
    act,
    hid,
    y_part,
    y_recv,
    z_send,
    z_recv,
    load_sems,
    part_sems,
    table_sems,
    scale_sems,
    dense_sems,
    row_sems,
    relay_sems,
    y_sems,
    z_sems,
):
    f32 = jnp.float32
    bf16 = jnp.bfloat16
    me_e = lax.axis_index("ep")
    me_t = lax.axis_index("tp")
    side = me_t // 2
    core = lax.rem(me_t, 2)
    count, width = tokens.shape
    own_width = width // tp_size
    total = ep_size * count
    hidden_width = dgate_hbm.shape[0]
    halves = tp_size // 2

    def remote(src, dst, send, recv, to_e, to_t):
        return pltpu.make_async_remote_copy(
            src_ref=src,
            dst_ref=dst,
            send_sem=send,
            recv_sem=recv,
            device_id=(to_e, to_t),
            device_id_type=pl.DeviceIdType.MESH,
        )

    barrier = pltpu.get_barrier_semaphore()
    for m in range(1, tp_size):
        pl.semaphore_signal(
            barrier,
            inc=1,
            device_id=(me_e, flip(me_t, m)),
            device_id_type=pl.DeviceIdType.MESH,
        )
    for m in range(ep_size - 1, 0, -1):
        pl.semaphore_signal(
            barrier,
            inc=1,
            device_id=(flip(me_e, m), me_t),
            device_id_type=pl.DeviceIdType.MESH,
        )

    def dense_rows(ref, t):
        if slice_rows == hidden_width:
            return ref
        return ref.at[pl.ds(t * slice_rows, slice_rows)]

    dense_hbm = [dgate_hbm, dup_hbm, ddown_hbm]
    loads = []
    for src, dst in [
        (rows_hbm, mrows),
        (outw_hbm, outw),
        (tokens_hbm, tokens),
        (gain_hbm, gain),
        (routes_hbm, routes),
        (rweights_hbm, rweights),
        (scale_hbm, scales.at[me_t]),
        (gate_hbm, gate_w),
        (up_hbm, up_w),
        (down_hbm, down_w),
        (dense_rows(dgate_hbm, me_t), dense_w.at[0, me_t]),
        (dense_rows(dup_hbm, me_t), dense_w.at[1, me_t]),
        (dense_rows(ddown_hbm, me_t), dense_w.at[2, me_t]),
    ]:
        copy = pltpu.make_async_copy(src, dst, load_sems.at[len(loads)])
        copy.start()
        loads.append(copy)

    loads[0].wait()
    loads[1].wait()
    mixer_rows = mrows[...]
    for q in range(tp_size):
        piece = dot(mixer_rows, outw[:, q * own_width : (q + 1) * own_width])
        part[q % 2, q // 2] = piece.astype(bf16)
    loads[4].wait()
    loads[5].wait()
    expert_of = lax.broadcasted_iota(jnp.int32, (ep_size, count), 0)
    table = jnp.zeros((ep_size, count), f32)
    for k in range(routes.shape[0]):
        table = table + jnp.where(expert_of == routes[k : k + 1, :], rweights[k : k + 1, :], 0.0)
    tables[me_e] = jnp.concatenate([table, jnp.zeros((ep_size, LANES - count), f32)], axis=1)
    loads[2].wait()
    loads[6].wait()

    pl.semaphore_wait(barrier, ep_size + tp_size - 2)
    tp_order = [m for m in range(2, tp_size)] + [1]
    part_copies = {}
    for m in tp_order:
        to = flip(me_t, m)
        part_copies[m] = remote(
            part.at[lax.rem(to, 2)],
            parts.at[m],
            part_sems.at[0, m],
            part_sems.at[1, m],
            me_e,
            to,
        )
        part_copies[m].start()
    table_copies = []
    for m in range(1, ep_size):
        copy = remote(
            tables.at[me_e],
            tables.at[me_e],
            table_sems.at[0, m],
            table_sems.at[1, m],
            flip(me_e, m),
            me_t,
        )
        copy.start()
        table_copies.append(copy)
    dense_copies = []
    for m in tp_order:
        to = flip(me_t, m)
        copy = remote(
            scales.at[me_t],
            scales.at[me_t],
            scale_sems.at[0, m],
            scale_sems.at[1, m],
            me_e,
            to,
        )
        copy.start()
        dense_copies.append(copy)
        for k in range(3):
            copy = remote(
                dense_rows(dense_hbm[k], to),
                dense_w.at[k, me_t],
                dense_sems.at[0, k, m],
                dense_sems.at[1, k, m],
                me_e,
                to,
            )
            copy.start()
            dense_copies.append(copy)

    own_rows = []
    for h in range(halves):
        at = pl.ds(pl.multiple_of(core * own_width + 2 * h * own_width, own_width), own_width)
        own_rows.append(tokens[:, at].astype(f32) + part[core, h].astype(f32))
    for m in [1] + tp_order[:-1]:
        part_copies[m].wait_recv()
        for h in range(halves):
            own_rows[h] = own_rows[h] + parts[m, h].astype(f32)
    for h in range(halves):
        residual[h] = own_rows[h]
        rows[core, me_e, h] = own_rows[h].astype(bf16)

    row_copies = {}
    for m in range(ep_size - 1, 0, -1):
        row_copies[m] = remote(
            rows.at[core, me_e],
            rows.at[core, me_e],
            row_sems.at[0, m],
            row_sems.at[1, m],
            flip(me_e, m),
            me_t,
        )
        row_copies[m].start()
    partner = flip(me_t, 1)
    relay_copies = {}
    for m in range(ep_size):
        origin = flip(me_e, m)
        if m:
            row_copies[m].wait_recv()
        relay_copies[m] = remote(
            rows.at[core, origin],
            rows.at[core, origin],
            relay_sems.at[0, m],
            relay_sems.at[1, m],
            me_e,
            partner,
        )
        relay_copies[m].start()
    loads[3].wait()
    for m in range(ep_size):
        origin = flip(me_e, m)
        relay_copies[m].wait_recv()
        pieces = [rows[q % 2, origin, q // 2].astype(f32) for q in range(tp_size)]
        squares = pieces[0] * pieces[0]
        for q in range(1, tp_size):
            squares = squares + pieces[q] * pieces[q]
        scale_of = lax.rsqrt(jnp.sum(squares, axis=-1, keepdims=True) * (1.0 / width) + eps)
        at = pl.ds(pl.multiple_of(origin * count, count), count)
        for q in range(tp_size):
            lanes = slice(q * own_width, (q + 1) * own_width)
            flat[at, lanes] = pieces[q] * scale_of * gain[:, lanes]
    packed[...] = flat[...].astype(bf16)

    for i in range(7, 13):
        loads[i].wait()
    for copy in table_copies + dense_copies:
        copy.wait_recv()

    groups = 8 if ep_size % 8 == 0 else ep_size
    chunk = groups * count
    expert_hidden = gate_w.shape[1]
    unit = 64 if expert_hidden % 64 == 0 else expert_hidden
    if slice_rows == hidden_width:
        units = lax.broadcasted_iota(jnp.int32, (slice_rows, 1), 0)
        share = hidden_width // tp_size
        kept = (units // share == me_t).astype(f32)

    def activate(step, carry):
        at = pl.ds(pl.multiple_of(step * chunk, chunk), chunk)
        x = packed[at, :]
        for n in range(0, expert_hidden, unit):
            gate_act = dot_rows(gate_w[0, n : n + unit, :], x)
            up_act = dot_rows(up_w[0, n : n + unit, :], x)
            act[step, n : n + unit, :] = (silu(gate_act) * up_act).astype(bf16)
        gate_act = jnp.zeros((slice_rows, chunk), f32)
        up_act = jnp.zeros((slice_rows, chunk), f32)
        for t in range(tp_size):
            x_part = packed[at, t * own_width : (t + 1) * own_width]
            gate_act = gate_act + dot_rows(dense_w[0, t], x_part)
            up_act = up_act + dot_rows(dense_w[1, t], x_part)
        hidden = silu(gate_act) * up_act
        if slice_rows == hidden_width:
            hidden = hidden * kept
        hid[step] = hidden.astype(bf16)
        return carry

    lax.fori_loop(0, total // chunk, activate, 0)

    def weigh(b):
        held = tables[b]
        mine = lax.broadcasted_iota(jnp.int32, held.shape, 0) == me_e
        row = jnp.sum(jnp.where(mine, held, 0.0), axis=0, keepdims=True)[:, :count]
        diagonal = lax.broadcasted_iota(jnp.int32, (count, count), 0) == lax.broadcasted_iota(
            jnp.int32, (count, count), 1
        )
        return jnp.sum(jnp.where(diagonal, row, 0.0), axis=1, keepdims=True)

    contract_rows = (((0,), (0,)), ((), ()))

    def project(step, carry):
        acts = act[step]
        hidden = hid[step]
        weights = [weigh(step * groups + g) for g in range(groups)]
        for q in range(tp_size):
            lanes = slice(q * own_width, (q + 1) * own_width)
            routed = lax.dot_general(
                acts, down_w[0, :, lanes], contract_rows, preferred_element_type=f32
            )
            dense = lax.dot_general(
                hidden, dense_w[2, q], contract_rows, preferred_element_type=f32
            )
            for g in range(groups):
                at = slice(g * count, (g + 1) * count)
                y = routed[at] * weights[g] + dense[at] * scales[q]
                y_part[q % 2, q // 2, step * groups + g] = y.astype(bf16)
        return carry

    lax.fori_loop(0, total // chunk, project, 0)

    y_copies = []
    half_blocks = ep_size // 2
    top = me_e // half_blocks
    for k in range(2):
        which = (1 - top) if k == 0 else top
        at = pl.ds(which * half_blocks, half_blocks)
        copy = remote(
            y_part.at[1 - core, :, at],
            y_recv.at[:, at],
            y_sems.at[0, k],
            y_sems.at[1, k],
            me_e,
            partner,
        )
        copy.start()
        y_copies.append(copy)
    z_copies = []
    for k in range(2):
        y_copies[k].wait_recv()
        for m in range(ep_size // 2 * (2 - k) - 1, ep_size // 2 * (1 - k) - 1, -1):
            to = flip(me_e, m)
            for o in range(halves - 1, -1, -1):
                to_side = flip(side, o)
                summed = y_part[core, to_side, to].astype(f32) + y_recv[to_side, to].astype(f32)
                if m == 0 and o == 0:
                    final = residual[side] + summed
                    continue
                z_send[to_side, to] = summed.astype(bf16)
                copy = remote(
                    z_send.at[to_side, to],
                    z_recv.at[side, me_e],
                    z_sems.at[0, o, m],
                    z_sems.at[1, o, m],
                    to,
                    2 * to_side + core,
                )
                copy.start()
                z_copies.append((m, o, copy))
    for m, o, copy in sorted(z_copies, key=lambda item: item[:2]):
        copy.wait_recv()
        final = final + z_recv[flip(side, o), flip(me_e, m)].astype(f32)
    out[...] = final.astype(bf16)
    for copies in [part_copies, row_copies, relay_copies]:
        for copy in copies.values():
            copy.wait_send()
    for copy in table_copies + dense_copies + y_copies:
        copy.wait_send()
    for m, o, copy in z_copies:
        copy.wait_send()


def local(
    tokens,
    mixer_gain,
    gate_weight,
    inner_weight,
    state_weight,
    step_weight,
    step_bias,
    decay_log,
    skip_scale,
    inner_kernel,
    state_kernel,
    inner_window,
    state_window,
    recurrent_state,
    group_gain,
    output_weight,
    channel_gain,
    routes,
    route_weights,
    expert_gate,
    expert_up,
    expert_down,
    dense_gate,
    dense_up,
    dense_down,
    dense_scale,
):
    f32 = jnp.float32
    bf16 = jnp.bfloat16
    ep_size = lax.axis_size("ep")
    tp_size = lax.axis_size("tp")
    count, width = tokens.shape
    own_width = width // tp_size
    total = ep_size * count
    hbm = pl.BlockSpec(memory_space=pl.ANY)
    dma = pltpu.SemaphoreType.DMA
    vmem = pltpu.VMEM
    steps = count // SEQ_STEP

    inner_window = jnp.swapaxes(inner_window, 0, 1)
    taps = inner_kernel.shape[0]
    inner = inner_weight.shape[1]
    mixer_args = [
        tokens,
        mixer_gain[None],
        gate_weight,
        inner_weight,
        state_weight,
        step_weight.T,
        step_bias[None],
        decay_log[None],
        skip_scale[None],
        inner_kernel,
        state_kernel,
        inner_window,
        state_window,
        recurrent_state,
        group_gain[None],
    ]
    held = [vmem(a.shape, a.dtype) for a in mixer_args]
    held[11] = vmem((taps,) + inner_window.shape[1:], bf16)
    held[12] = vmem((count, taps) + state_window.shape[2:], bf16)
    heads = step_bias.shape[0]
    n_state = state_weight.shape[2]
    mixer_rows, new_state, new_inner, new_state_window = pl.pallas_call(
        mixer,
        out_shape=[
            jax.ShapeDtypeStruct((count, inner), bf16),
            jax.ShapeDtypeStruct(recurrent_state.shape, f32),
            jax.ShapeDtypeStruct(inner_window.shape, bf16),
            jax.ShapeDtypeStruct(state_window.shape, bf16),
        ],
        in_specs=[hbm] * len(mixer_args),
        out_specs=[hbm] * 4,
        scratch_shapes=held
        + [
            vmem((count, heads * n_state), f32),
            vmem((count, inner), f32),
            vmem((count, inner), bf16),
            dma((14,)),
            dma((2, steps)),
            dma((3,)),
        ],
        compiler_params=pltpu.CompilerParams(vmem_limit_bytes=60 * 1024 * 1024),
    )(*mixer_args)

    expert_gate = jnp.swapaxes(expert_gate, 1, 2)
    expert_up = jnp.swapaxes(expert_up, 1, 2)
    hidden_width = dense_gate.shape[1]
    slice_rows = hidden_width // tp_size
    if hidden_width % (8 * tp_size):
        slice_rows = hidden_width
    halves = tp_size // 2
    groups = 8 if ep_size % 8 == 0 else ep_size
    chunk = groups * count
    branch_args = [
        mixer_rows,
        output_weight,
        tokens,
        channel_gain[None],
        routes.T,
        route_weights.T,
        dense_scale[None],
        expert_gate,
        expert_up,
        expert_down,
        dense_gate.T,
        dense_up.T,
        dense_down,
    ]
    new_tokens = pl.pallas_call(
        functools.partial(branches, ep_size, tp_size, slice_rows),
        out_shape=jax.ShapeDtypeStruct((count, own_width), bf16),
        in_specs=[hbm] * len(branch_args),
        out_specs=pl.BlockSpec(memory_space=pltpu.VMEM),
        scratch_shapes=[vmem(a.shape, a.dtype) for a in branch_args[:6]]
        + [
            vmem((tp_size, 1, own_width), f32),
            vmem(expert_gate.shape, bf16),
            vmem(expert_up.shape, bf16),
            vmem(expert_down.shape, bf16),
            vmem((3, tp_size, slice_rows, own_width), bf16),
            vmem((ep_size, ep_size, LANES), f32),
            vmem((2, halves, count, own_width), bf16),
            vmem((tp_size, halves, count, own_width), bf16),
            vmem((halves, count, own_width), f32),
            vmem((2, ep_size, halves, count, own_width), bf16),
            vmem((total, width), f32),
            vmem((total, width), bf16),
            vmem((total // chunk, expert_gate.shape[1], chunk), bf16),
            vmem((total // chunk, slice_rows, chunk), bf16),
            vmem((2, halves, ep_size, count, own_width), bf16),
            vmem((halves, ep_size, count, own_width), bf16),
            vmem((halves, ep_size, count, own_width), bf16),
            vmem((halves, ep_size, count, own_width), bf16),
            dma((13,)),
            dma((2, tp_size)),
            dma((2, ep_size)),
            dma((2, tp_size)),
            dma((2, 3, tp_size)),
            dma((2, ep_size)),
            dma((2, ep_size)),
            dma((2, 2)),
            dma((2, halves, ep_size)),
        ],
        compiler_params=pltpu.CompilerParams(
            collective_id=0, has_side_effects=True, vmem_limit_bytes=60 * 1024 * 1024
        ),
    )(*branch_args)
    return (
        new_tokens,
        new_state,
        jnp.swapaxes(new_inner, 0, 1),
        new_state_window,
    )


def solution(mesh):
    placed = (
        P("ep", None),
        P(),
        P(None, "tp"),
        P(None, "tp"),
        P(None, None, "tp"),
        P(None, "tp"),
        P("tp"),
        P("tp"),
        P("tp"),
        P(None, "tp"),
        P(None, None, "tp"),
        P("ep", None, "tp"),
        P("ep", None, None, "tp"),
        P("ep", "tp", None, None),
        P("tp"),
        P("tp", None),
        P(),
        P("ep", None),
        P("ep", None),
        P("ep", None, "tp"),
        P("ep", None, "tp"),
        P("ep", "tp", None),
        P("tp", "ep"),
        P("tp", "ep"),
        P("ep", "tp"),
        P("tp"),
    )
    return jax.shard_map(
        local,
        mesh=mesh,
        in_specs=placed,
        out_specs=(
            P("ep", "tp"),
            P("ep", "tp", None, None),
            P("ep", None, "tp"),
            P("ep", None, None, "tp"),
        ),
        check_vma=False,
    )
```

time: 55.8 us -> 37 us (0.66); the launches traced: 54.7 us -> 36.6 us
  other arithmetic: 8.35 us -> 0 us
  matrix products: 5.97 us -> 0 us
  local copies, waits for them, and re-layouts: 4.01 us -> 1.31 us
  Pallas kernels: 35.6 us -> 34.7 us
    reduce_sum x5 -> x0, other arithmetic: 7.57 us -> none  [the longest x1 4.36 us: local(): mixed_out = jnp.sum(new_state * out_vector[:, :, None, None, :], axis=-1)]
    dot_general x6 -> x0, matrix products: 5.97 us -> none  [the longest x1 1.32 us: local(): jnp.dot(normed, inner_weight, preferred_element_type=f32).astype(bf16)]
    pallas_call x1 -> x2, Pallas kernels: 35.6 us -> 34.7 us  [the longest x1 28.9 us: local(): pl.pallas_call(functools.partial(branches, ep_size, tp_size, slice_rows),...]
    unnamed x20 -> x1, local copies, waits for them, and re-layouts: 2.15 us -> 1.31 us
    exp x2 -> x0, local copies, waits for them, and re-layouts: 0.75 us -> none  [local(): decay_rate = jnp.exp(-step_size * jnp.exp(decay_log))]
    slice x2 -> x0, local copies, waits for them, and re-layouts: 0.66 us -> none  [the longest x1 0.64 us: local(): state_ctx[:, 1:]]
    concatenate x1 -> x0, other arithmetic: 0.62 us -> none  [local(): inner_ctx = jnp.concatenate([inner_window, inner_pre[:, None, :]], axis=1)]
where the time goes in v1:
time: 37 us; the launch traced here: 36.6 us
  Pallas kernels  34.7 us (94%)
  local copies, waits for them, and re-layouts  1.31 us (4%)
  between operations  0.65 us (2%)
    pallas_call x1, Pallas kernels, local(): pl.pallas_call(functools.partial(branches, ep_size, tp_size, slice_rows),...  28.9 us
    pallas_call x1, Pallas kernels, local(): pl.pallas_call(mixer, out_shape=[jax.ShapeDtypeStruct((count, inner), bf1...  5.83 us
    unnamed x1, local copies, waits for them, and re-layouts  1.31 us

profile of v1, /device:TPU:0, one launch (start us, length us, event | category | flops | bytes accessed | tf_op | source)
XLA Modules:
  0.0 36.6 jit_solution(11343831135892617229)
XLA Ops:
  0.6 5.8 %shard_map.273 = (bf16[24,256]{1,0:T(8,128)(2,1)}, f32[24,4,64,128]{3,2,1,0:T(8,128)}, bf16[3,24,256]{2,1,0:T(8,128)(2,1)}, bf16[24,3,2,128]{3,2,1,0:T(2,128)(2,1)}) custom-call(bf16[24,1024]{1,0:T(8,128)(2,1)} %tokens_hbm.3, f32[1,1024]{1,0:T(1,128)} %bitcast.23, bf16[1024,256]{1,0:T(8,128)(2,1)} %gatew_hbm.1, bf16[1024,256]{1,0:T(8,128)(2,1)} %innerw_hbm.1, ...), custom_call_target="tpu_custom_call" | custom-call | tf_op jit(solution)/shard_map/pallas_call | solution.py:638
  6.5 28.9 %shard_map.274 = bf16[24,256]{1,0:T(8,128)(2,1)} custom-call(bf16[24,256]{1,0:T(8,128)(2,1)} %get-tuple-element.8.rows_hbm, bf16[256,1024]{1,0:T(8,128)(2,1)} %outw_hbm.1, bf16[24,1024]{1,0:T(8,128)(2,1)} %tokens_hbm.3, f32[1,1024]{1,0:T(1,128)} %bitcast.22, s32[2,24]{1,0:T(2,128)} %bitcast.24, f32[2,24]{1,0:T(2,128)} %bitcast.25, f32[1,256]{1,0:T(1,128)} %bitcast.26, ...), custom_call_target="tpu_custom_call" | custom-call | tf_op jit(solution)/shard_map/pallas_call | solution.py:684
  35.3 1.3 %copy.31 = bf16[24,256]{1,0:T(8,128)(2,1)} copy(bf16[24,256]{1,0:T(8,128)(2,1)} %shard_map.274) | data formatting | bytes 24576

commit v2 on v1

v2 whole, which is shorter than its diff:
```python
import functools

import jax
import jax.numpy as jnp
from jax import lax
from jax.experimental import pallas as pl
from jax.experimental.pallas import tpu as pltpu
from jax.sharding import PartitionSpec as P

HEADS = 16
GROUPS = 4
HEAD_DIM = 64
STATE_DIM = 128
LANES = 128
SEQ_STEP = 4
ROW_ORDER = (7, 6, 5, 4, 3, 2, 1)

eps = 1e-06


def silu(v):
    return v / (1.0 + jnp.exp(-v))


def dot_rows(rows, columns):
    return lax.dot_general(
        rows, columns, (((1,), (1,)), ((), ())), preferred_element_type=jnp.float32
    )


def dot(a, b):
    return jnp.dot(a, b, preferred_element_type=jnp.float32)


def mixer(
    tokens_hbm,
    mgain_hbm,
    gatew_hbm,
    innerw_hbm,
    statew_hbm,
    stepw_hbm,
    sbias_hbm,
    dlog_hbm,
    skip_hbm,
    ikern_hbm,
    skern_hbm,
    iwin_hbm,
    swin_hbm,
    state_hbm,
    ggain_hbm,
    rows_out,
    state_out,
    iwin_out,
    swin_out,
    tokens,
    mgain,
    gatew,
    innerw,
    statew,
    stepw,
    sbias,
    dlog,
    skip,
    ikern,
    skern,
    iwin,
    swin,
    state,
    ggain,
    decays,
    mixed,
    sems,
    state_sems,
    out_sems,
):
    f32 = jnp.float32
    bf16 = jnp.bfloat16
    count = tokens.shape[0]
    taps = ikern.shape[0]
    heads = sbias.shape[1]
    inner = innerw.shape[1]
    head_dim = inner // heads
    n_state = statew.shape[2]
    small = [
        (tokens_hbm, tokens),
        (mgain_hbm, mgain),
        (innerw_hbm, innerw),
        (statew_hbm, statew),
        (stepw_hbm, stepw),
        (sbias_hbm, sbias),
        (dlog_hbm, dlog),
        (ikern_hbm, ikern),
        (skern_hbm, skern),
        (iwin_hbm, iwin.at[pl.ds(0, taps - 1)]),
        (swin_hbm, swin.at[:, pl.ds(0, taps - 1)]),
        (gatew_hbm, gatew),
        (skip_hbm, skip),
        (ggain_hbm, ggain),
    ]
    loads = []
    for i, (src, dst) in enumerate(small):
        copy = pltpu.make_async_copy(src, dst, sems.at[i])
        copy.start()
        loads.append(copy)

    def state_load(i):
        at = pl.ds(i * SEQ_STEP, SEQ_STEP)
        return pltpu.make_async_copy(state_hbm.at[at], state.at[at], state_sems.at[0, i])

    def state_store(i):
        at = pl.ds(i * SEQ_STEP, SEQ_STEP)
        return pltpu.make_async_copy(state.at[at], state_out.at[at], state_sems.at[1, i])

    steps = count // SEQ_STEP
    loads[0].wait()
    loads[1].wait()
    for i in range(steps):
        state_load(i).start()
    value = tokens[...].astype(f32)
    squares = jnp.mean(value * value, axis=-1, keepdims=True)
    normed = (value * lax.rsqrt(squares + eps) * mgain[...]).astype(bf16)
    for i in range(2, 14):
        loads[i].wait()
    inner_pre = dot(normed, innerw[...]).astype(bf16)
    pre_u = dot(normed, statew[0])
    pre_c = dot(normed, statew[1])
    step_raw = dot_rows(normed, stepw[...])
    gate_pre = dot(normed, gatew[...])

    iwin[taps - 1] = inner_pre
    conv = inner_pre.astype(f32) * ikern[taps - 1 : taps, :]
    for j in range(taps - 1):
        conv = conv + iwin[j].astype(f32) * ikern[j : j + 1, :]
    inner_conv = silu(conv)

    both = jnp.concatenate([pre_u[:, None, :], pre_c[:, None, :]], axis=1).astype(bf16)
    swin[:, taps - 1] = both
    sconv = both.astype(f32) * skern[taps - 1][None]
    for j in range(taps - 1):
        sconv = sconv + swin[:, j].astype(f32) * skern[j][None]
    sconv = silu(sconv)
    u_vec = sconv[:, 0, :]
    c_vec = sconv[:, 1, :]
    win_copies = [
        pltpu.make_async_copy(iwin.at[pl.ds(1, taps - 1)], iwin_out, out_sems.at[0]),
        pltpu.make_async_copy(swin.at[:, pl.ds(1, taps - 1)], swin_out, out_sems.at[1]),
    ]
    for copy in win_copies:
        copy.start()

    step_size = jax.nn.softplus(step_raw + sbias[...])
    decay = jnp.exp(-step_size * jnp.exp(dlog[...]))
    step_wide = jnp.concatenate(
        [jnp.broadcast_to(step_size[:, h : h + 1], (count, head_dim)) for h in range(heads)],
        axis=1,
    )
    decay_wide = jnp.concatenate(
        [jnp.broadcast_to(decay[:, h : h + 1], (count, head_dim)) for h in range(heads)], axis=1
    )
    for h in range(heads):
        decays[:, h * n_state : (h + 1) * n_state] = jnp.broadcast_to(
            decay[:, h : h + 1], (count, n_state)
        )
    moved = step_wide * inner_conv
    written = moved.T.astype(bf16)
    row_of = lax.broadcasted_iota(jnp.int32, (count, n_state), 0)
    lane_of = lax.broadcasted_iota(jnp.int32, (inner, 2 * count), 1)
    none = jnp.zeros_like(c_vec)
    readers = jnp.concatenate(
        [jnp.concatenate([c_vec, none], axis=1), jnp.concatenate([none, c_vec], axis=1)], axis=0
    ).astype(bf16)

    for i in range(steps):
        state_load(i).wait()
        for b in range(i * SEQ_STEP, (i + 1) * SEQ_STEP, 2):
            pair = jnp.concatenate(
                [jnp.where(row_of == b + n, u_vec, 0.0) for n in range(2)], axis=1
            ).astype(bf16)
            outer = dot(written, pair)
            old = [
                jnp.concatenate([state[b + n, h].astype(bf16) for h in range(heads)], axis=0)
                for n in range(2)
            ]
            read = dot_rows(jnp.concatenate(old, axis=1), readers)
            if b:
                read = jnp.where((lane_of == b) | (lane_of == count + b + 1), read, mixed[...])
            mixed[...] = read
            for n in range(2):
                for h in range(heads):
                    fade = decays[b + n : b + n + 1, h * n_state : (h + 1) * n_state]
                    state[b + n, h] = (
                        state[b + n, h] * fade
                        + outer[h * head_dim : (h + 1) * head_dim, n * n_state : (n + 1) * n_state]
                    )
        state_store(i).start()

    read = mixed[...].T
    even = lax.rem(lax.broadcasted_iota(jnp.int32, (count, inner), 0), 2) == 0
    read = jnp.where(even, read[:count], read[count:])
    mixed_out = decay_wide * read + moved * jnp.sum(u_vec * c_vec, axis=1, keepdims=True)
    skip_wide = jnp.concatenate(
        [jnp.broadcast_to(skip[:, h : h + 1], (1, head_dim)) for h in range(heads)], axis=1
    )
    gated = (mixed_out + skip_wide * inner_conv) * silu(gate_pre)
    squares = jnp.mean(gated * gated, axis=-1, keepdims=True)
    rows_out[...] = (gated * lax.rsqrt(squares + eps) * ggain[...]).astype(bf16)
    for i in range(steps):
        state_store(i).wait()
    for copy in win_copies:
        copy.wait()


def padded(rows):
    return -(-rows // 16) * 16


def flipped(a, b):
    low = lax.rem(a + b, 2)
    high = lax.rem(a // 2 + b // 2, 2)
    return 2 * high + low


def flip(index, mask):
    moved = index
    bit = 1
    while bit <= mask:
        if mask & bit:
            moved = moved + bit * (1 - 2 * lax.rem(index // bit, 2))
        bit *= 2
    return moved


def branches(
    ep_size,
    tp_size,
    slice_rows,
    chunks,
    mrows,
    outw,
    tokens,
    gain,
    routes,
    rweights,
    scale,
    gate_hbm,
    up_hbm,
    down_hbm,
    dgate_hbm,
    dup_hbm,
    ddown_hbm,
    out,
    scales,
    weights_in,
    down_w,
    dense_w,
    tables,
    part,
    parts,
    residual,
    rows,
    flat,
    pre,
    act,
    y_part,
    y_recv,
    z_send,
    z_recv,
    load_sems,
    part_sems,
    table_sems,
    scale_sems,
    dense_sems,
    row_send,
    row_sems,
    relay_send,
    relay_sems,
    y_sems,
    z_sems,
):
    f32 = jnp.float32
    bf16 = jnp.bfloat16
    me_e = lax.axis_index("ep")
    me_t = lax.axis_index("tp")
    side = me_t // 2
    core = lax.rem(me_t, 2)
    partner = flip(me_t, 1)
    count, width = tokens.shape
    own_width = width // tp_size
    hidden_width = dgate_hbm.shape[0]
    halves = tp_size // 2
    expert_hidden = gate_hbm.shape[1]
    dense_at = [2 * expert_hidden, 2 * expert_hidden + padded(slice_rows)]

    def remote(src, dst, send, recv, to_e, to_t):
        copy = pltpu.make_async_remote_copy(
            src_ref=src,
            dst_ref=dst,
            send_sem=send,
            recv_sem=recv,
            device_id=(to_e, to_t),
            device_id_type=pl.DeviceIdType.MESH,
        )
        copy.start()
        return copy

    def settle(ref, sem):
        pltpu.make_async_copy(ref, ref, sem).wait()

    barrier = pltpu.get_barrier_semaphore()
    for m in range(1, tp_size):
        pl.semaphore_signal(
            barrier,
            inc=1,
            device_id=(me_e, flip(me_t, m)),
            device_id_type=pl.DeviceIdType.MESH,
        )
    for m in range(ep_size - 1, 0, -1):
        pl.semaphore_signal(
            barrier,
            inc=1,
            device_id=(flip(me_e, m), me_t),
            device_id_type=pl.DeviceIdType.MESH,
        )

    def dense_rows(ref, t):
        if slice_rows == hidden_width:
            return ref
        return ref.at[pl.ds(t * slice_rows, slice_rows)]

    dense_hbm = [dgate_hbm, dup_hbm, ddown_hbm]
    for src, dst, sem in [
        (gate_hbm.at[0], weights_in.at[pl.ds(0, expert_hidden)], 0),
        (up_hbm.at[0], weights_in.at[pl.ds(expert_hidden, expert_hidden)], 0),
        (down_hbm.at[0], down_w, 1),
    ] + [(dense_rows(dense_hbm[k], me_t), dense_w.at[0, k], 2) for k in range(3)]:
        pltpu.make_async_copy(src, dst, load_sems.at[sem]).start()

    mixer_rows = mrows[...]
    for q in range(tp_size):
        piece = dot(mixer_rows, outw[:, q * own_width : (q + 1) * own_width])
        part[q % 2, q // 2] = piece.astype(bf16)
    expert_of = lax.broadcasted_iota(jnp.int32, (ep_size, count), 0)
    table = jnp.zeros((ep_size, count), f32)
    for k in range(routes.shape[0]):
        table = table + jnp.where(expert_of == routes[k : k + 1, :], rweights[k : k + 1, :], 0.0)
    tables[0] = jnp.concatenate([table, jnp.zeros((ep_size, LANES - count), f32)], axis=1)
    scales[0] = scale[...]

    pl.semaphore_wait(barrier, ep_size + tp_size - 2)
    tp_order = [m for m in range(2, tp_size)] + [1]
    for m in tp_order:
        to = flip(me_t, m)
        remote(
            part.at[lax.rem(to, 2)], parts.at[m], part_sems.at[0], part_sems.at[1], me_e, to
        )
    for m in range(1, ep_size):
        remote(
            tables.at[0], tables.at[m], table_sems.at[0], table_sems.at[1], flip(me_e, m), me_t
        )
    for m in tp_order:
        to = flip(me_t, m)
        remote(scales.at[0], scales.at[m], scale_sems.at[0], scale_sems.at[1], me_e, to)
        for k in range(3):
            remote(
                dense_rows(dense_hbm[k], to),
                dense_w.at[m, k],
                dense_sems.at[0],
                dense_sems.at[1],
                me_e,
                to,
            )

    own_rows = []
    for h in range(halves):
        at = pl.ds(pl.multiple_of(core * own_width + 2 * h * own_width, own_width), own_width)
        own_rows.append(tokens[:, at].astype(f32) + part[core, h].astype(f32))
    settle(parts.at[pl.ds(1, tp_size - 1)], part_sems.at[1])
    for h in range(halves):
        for m in range(1, tp_size):
            own_rows[h] = own_rows[h] + parts[m, h].astype(f32)
        residual[h] = own_rows[h]
        rows[core, 0, h] = own_rows[h].astype(bf16)

    row_copies = {}
    for m in ROW_ORDER if ep_size == 8 else range(1, ep_size):
        row_copies[m] = remote(
            rows.at[core, 0],
            rows.at[core, m],
            row_send.at[0],
            row_sems.at[m],
            flip(me_e, m),
            me_t,
        )

    relay_copies = {}

    def relay(m):
        if m:
            row_copies[m].wait_recv()
        relay_copies[m] = remote(
            rows.at[core, m],
            rows.at[core, m],
            relay_send.at[0],
            relay_sems.at[m],
            me_e,
            partner,
        )

    def normalize(m, at):
        relay_copies[m].wait_recv()
        pieces = [rows[q % 2, m, q // 2].astype(f32) for q in range(tp_size)]
        squares = pieces[0] * pieces[0]
        for q in range(1, tp_size):
            squares = squares + pieces[q] * pieces[q]
        scale_of = lax.rsqrt(jnp.sum(squares, axis=-1, keepdims=True) * (1.0 / width) + eps)
        for q in range(tp_size):
            lanes = slice(q * own_width, (q + 1) * own_width)
            flat[at * count : (at + 1) * count, lanes] = pieces[q] * scale_of * gain[:, lanes]

    unit = 64 if expert_hidden % 64 == 0 else expert_hidden
    if slice_rows == hidden_width:
        units = lax.broadcasted_iota(jnp.int32, (slice_rows, 1), 0)
        share = hidden_width // tp_size
        kept = (units // share == me_t).astype(f32)

    def place_weights():
        settle(weights_in.at[pl.ds(0, 2 * expert_hidden)], load_sems.at[0])
        settle(down_w, load_sems.at[1])
        settle(dense_w.at[0], load_sems.at[2])
        settle(tables.at[pl.ds(1, ep_size - 1)], table_sems.at[1])
        settle(scales.at[pl.ds(1, tp_size - 1)], scale_sems.at[1])
        settle(dense_w.at[pl.ds(1, tp_size - 1)], dense_sems.at[1])
        for k in range(2):
            at = slice(dense_at[k], dense_at[k] + slice_rows)
            for m in range(tp_size):
                lanes = pl.ds(pl.multiple_of(flip(me_t, m) * own_width, own_width), own_width)
                weights_in[at, lanes] = dense_w[m, k]

    def activate(chunk):
        live = len(chunk) * count
        lanes = slice(0, live)
        x = flat[:live, :].astype(bf16)
        pre[:, lanes] = dot_rows(weights_in[...], x)
        for n in range(0, expert_hidden, unit):
            gate_act = pre[n : n + unit, lanes]
            up_act = pre[expert_hidden + n : expert_hidden + n + unit, lanes]
            act[n : n + unit, lanes] = (silu(gate_act) * up_act).astype(bf16)
        gate_act = pre[dense_at[0] : dense_at[0] + slice_rows, lanes]
        up_act = pre[dense_at[1] : dense_at[1] + slice_rows, lanes]
        hidden = silu(gate_act) * up_act
        if slice_rows == hidden_width:
            hidden = hidden * kept
        act[expert_hidden : expert_hidden + slice_rows, lanes] = hidden.astype(bf16)

    def weigh(m):
        held = tables[m]
        mine = lax.broadcasted_iota(jnp.int32, held.shape, 0) == me_e
        row = jnp.sum(jnp.where(mine, held, 0.0), axis=0, keepdims=True)[:, :count]
        diagonal = lax.broadcasted_iota(jnp.int32, (count, count), 0) == lax.broadcasted_iota(
            jnp.int32, (count, count), 1
        )
        return jnp.sum(jnp.where(diagonal, row, 0.0), axis=1, keepdims=True)

    contract_rows = (((0,), (0,)), ((), ()))

    def project(chunk, first):
        live = len(chunk) * count
        weights = [weigh(m) for m in chunk]
        acts = act[:expert_hidden, :live]
        hidden = act[expert_hidden : expert_hidden + slice_rows, :live]
        sent = None
        for mine in range(2):
            whose = core if mine else 1 - core
            for h in range(halves):
                t = 2 * h + whose
                lanes = pl.ds(pl.multiple_of(t * own_width, own_width), own_width)
                slot = flipped(me_t, t)
                routed = lax.dot_general(
                    acts, down_w[:, lanes], contract_rows, preferred_element_type=f32
                )
                dense = lax.dot_general(
                    hidden, dense_w[slot, 2], contract_rows, preferred_element_type=f32
                )
                for g in range(len(chunk)):
                    at = slice(g * count, (g + 1) * count)
                    y = routed[at] * weights[g] + dense[at] * scales[slot]
                    y_part[mine, h, first + g] = y.astype(bf16)
            if not mine:
                at = pl.ds(first, len(chunk))
                sent = remote(
                    y_part.at[0, :, at],
                    y_recv.at[:, at],
                    y_sems.at[0, len(y_copies)],
                    y_sems.at[1, len(y_copies)],
                    me_e,
                    partner,
                )
        y_copies.append(sent)

    def give_back(chunk, first, sent):
        sent.wait_recv()
        kept_sum = None
        for g in reversed(range(len(chunk))):
            m = chunk[g]
            for o in range(halves - 1, -1, -1):
                to_side = flip(side, o)
                summed = y_part[1, to_side, first + g].astype(f32)
                summed = summed + y_recv[to_side, first + g].astype(f32)
                if m == 0 and o == 0:
                    kept_sum = summed
                    continue
                z_send[o * ep_size + m] = summed.astype(bf16)
                remote(
                    z_send.at[o * ep_size + m],
                    z_recv.at[o * ep_size + m],
                    z_sems.at[0],
                    z_sems.at[1],
                    flip(me_e, m),
                    2 * to_side + core,
                )
        return kept_sum

    y_copies = []
    firsts = [sum(len(c) for c in chunks[:k]) for k in range(len(chunks))]
    for m in chunks[0]:
        relay(m)
    for at, m in enumerate(chunks[0]):
        normalize(m, at)
    place_weights()
    activate(chunks[0])
    final = None
    for k, chunk in enumerate(chunks):
        after = chunks[k + 1] if k + 1 < len(chunks) else []
        for m in after:
            relay(m)
        project(chunk, firsts[k])
        for at, m in enumerate(after):
            normalize(m, at)
        if after:
            activate(after)
        kept_sum = give_back(chunk, firsts[k], y_copies[k])
        if kept_sum is not None:
            final = residual[side] + kept_sum

    settle(z_recv.at[pl.ds(1, halves * ep_size - 1)], z_sems.at[1])
    for o in range(halves):
        for m in range(ep_size):
            if m or o:
                final = final + z_recv[o * ep_size + m].astype(f32)
    out[...] = final.astype(bf16)

    settle(parts.at[pl.ds(1, tp_size - 1)], part_sems.at[0])
    settle(tables.at[pl.ds(1, ep_size - 1)], table_sems.at[0])
    settle(scales.at[pl.ds(1, tp_size - 1)], scale_sems.at[0])
    settle(dense_w.at[pl.ds(1, tp_size - 1)], dense_sems.at[0])
    settle(rows.at[0, pl.ds(1, ep_size - 1)], row_send.at[0])
    settle(rows.at[0], relay_send.at[0])
    for copy in y_copies:
        copy.wait_send()
    settle(z_send.at[pl.ds(1, halves * ep_size - 1)], z_sems.at[0])


def local(
    tokens,
    mixer_gain,
    gate_weight,
    inner_weight,
    state_weight,
    step_weight,
    step_bias,
    decay_log,
    skip_scale,
    inner_kernel,
    state_kernel,
    inner_window,
    state_window,
    recurrent_state,
    group_gain,
    output_weight,
    channel_gain,
    routes,
    route_weights,
    expert_gate,
    expert_up,
    expert_down,
    dense_gate,
    dense_up,
    dense_down,
    dense_scale,
):
    f32 = jnp.float32
    bf16 = jnp.bfloat16
    ep_size = lax.axis_size("ep")
    tp_size = lax.axis_size("tp")
    count, width = tokens.shape
    own_width = width // tp_size
    hbm = pl.BlockSpec(memory_space=pltpu.HBM)
    on_chip = pl.BlockSpec(memory_space=pltpu.VMEM)
    dma = pltpu.SemaphoreType.DMA
    vmem = pltpu.VMEM
    steps = count // SEQ_STEP

    inner_window = jnp.swapaxes(inner_window, 0, 1)
    taps = inner_kernel.shape[0]
    inner = inner_weight.shape[1]
    mixer_args = [
        tokens,
        mixer_gain[None],
        gate_weight,
        inner_weight,
        state_weight,
        step_weight.T,
        step_bias[None],
        decay_log[None],
        skip_scale[None],
        inner_kernel,
        state_kernel,
        inner_window,
        state_window,
        recurrent_state,
        group_gain[None],
    ]
    held = [vmem(a.shape, a.dtype) for a in mixer_args]
    held[11] = vmem((taps,) + inner_window.shape[1:], bf16)
    held[12] = vmem((count, taps) + state_window.shape[2:], bf16)
    heads = step_bias.shape[0]
    n_state = state_weight.shape[2]
    mixer_rows, new_state, new_inner, new_state_window = pl.pallas_call(
        mixer,
        out_shape=[
            jax.ShapeDtypeStruct((count, inner), bf16),
            jax.ShapeDtypeStruct(recurrent_state.shape, f32),
            jax.ShapeDtypeStruct(inner_window.shape, bf16),
            jax.ShapeDtypeStruct(state_window.shape, bf16),
        ],
        in_specs=[hbm] * len(mixer_args),
        out_specs=[on_chip] + [hbm] * 3,
        scratch_shapes=held
        + [
            vmem((count, heads * n_state), f32),
            vmem((inner, 2 * count), f32),
            dma((14,)),
            dma((2, steps)),
            dma((2,)),
        ],
        compiler_params=pltpu.CompilerParams(vmem_limit_bytes=24 * 1024 * 1024),
    )(*[pltpu.with_memory_space_constraint(a, pltpu.HBM) for a in mixer_args])

    expert_gate = jnp.swapaxes(expert_gate, 1, 2)
    expert_up = jnp.swapaxes(expert_up, 1, 2)
    hidden_width = dense_gate.shape[1]
    expert_hidden = expert_gate.shape[1]
    slice_rows = hidden_width // tp_size
    if hidden_width % (8 * tp_size):
        slice_rows = hidden_width
    halves = tp_size // 2
    chunk_len = min(ep_size, 4 if ep_size <= 8 else 8)
    chunks = [list(range(k, k + chunk_len)) for k in range(0, ep_size, chunk_len)]
    live = chunk_len * count
    wide = 2 * (expert_hidden + padded(slice_rows))
    branch_args = [
        mixer_rows,
        output_weight,
        tokens,
        channel_gain[None],
        routes.T,
        route_weights.T,
        dense_scale[None],
        expert_gate,
        expert_up,
        expert_down,
        dense_gate.T,
        dense_up.T,
        dense_down,
    ]
    new_tokens = pl.pallas_call(
        functools.partial(branches, ep_size, tp_size, slice_rows, chunks),
        out_shape=jax.ShapeDtypeStruct((count, own_width), bf16),
        in_specs=[on_chip] * 7 + [hbm] * (len(branch_args) - 7),
        out_specs=pl.BlockSpec(memory_space=pltpu.VMEM),
        scratch_shapes=[
            vmem((tp_size, 1, own_width), f32),
            vmem((wide, width), bf16),
            vmem(expert_down.shape[1:], bf16),
            vmem((tp_size, 3, slice_rows, own_width), bf16),
            vmem((ep_size, ep_size, LANES), f32),
            vmem((2, halves, count, own_width), bf16),
            vmem((tp_size, halves, count, own_width), bf16),
            vmem((halves, count, own_width), f32),
            vmem((2, ep_size, halves, count, own_width), bf16),
            vmem((live, width), f32),
            vmem((wide, live), f32),
            vmem((expert_hidden + padded(slice_rows), live), bf16),
            vmem((2, halves, ep_size, count, own_width), bf16),
            vmem((halves, ep_size, count, own_width), bf16),
            vmem((halves * ep_size, count, own_width), bf16),
            vmem((halves * ep_size, count, own_width), bf16),
            dma((3,)),
            dma((2,)),
            dma((2,)),
            dma((2,)),
            dma((2,)),
            dma((1,)),
            dma((ep_size,)),
            dma((1,)),
            dma((ep_size,)),
            dma((2, len(chunks))),
            dma((2,)),
        ],
        compiler_params=pltpu.CompilerParams(
            collective_id=0, has_side_effects=True, vmem_limit_bytes=(24 if ep_size <= 8 else 56) * 1024 * 1024
        ),
    )(*branch_args[:7], *[pltpu.with_memory_space_constraint(a, pltpu.HBM) for a in branch_args[7:]])
    return (
        new_tokens,
        new_state,
        jnp.swapaxes(new_inner, 0, 1),
        new_state_window,
    )


def solution(mesh):
    placed = (
        P("ep", None),
        P(),
        P(None, "tp"),
        P(None, "tp"),
        P(None, None, "tp"),
        P(None, "tp"),
        P("tp"),
        P("tp"),
        P("tp"),
        P(None, "tp"),
        P(None, None, "tp"),
        P("ep", None, "tp"),
        P("ep", None, None, "tp"),
        P("ep", "tp", None, None),
        P("tp"),
        P("tp", None),
        P(),
        P("ep", None),
        P("ep", None),
        P("ep", None, "tp"),
        P("ep", None, "tp"),
        P("ep", "tp", None),
        P("tp", "ep"),
        P("tp", "ep"),
        P("ep", "tp"),
        P("tp"),
    )
    return jax.shard_map(
        local,
        mesh=mesh,
        in_specs=placed,
        out_specs=(
            P("ep", "tp"),
            P("ep", "tp", None, None),
            P("ep", None, "tp"),
            P("ep", None, None, "tp"),
        ),
        check_vma=False,
    )
```

time: 37 us -> 34.8 us (0.941)
  Pallas kernels: 34.7 us -> 33.3 us
  local copies, waits for them, and re-layouts: 1.31 us -> 0.63 us
    pallas_call x1, Pallas kernels: 5.83 us -> 4.85 us  [local(): pl.pallas_call(mixer, out_shape=[jax.ShapeDtypeStruct((count, inner), bf1...]
    unnamed x1 -> x13, local copies, waits for them, and re-layouts: 1.31 us -> 0.63 us
    pallas_call x1, Pallas kernels: 28.9 us -> 28.4 us  [local(): pl.pallas_call(functools.partial(branches, ep_size, tp_size, slice_rows,...]
where the time goes in v2:
time: 34.8 us; the launch traced here: 34.7 us
  Pallas kernels  33.3 us (96%)
  between operations  0.75 us (2%)
  local copies, waits for them, and re-layouts  0.63 us (2%)
    pallas_call x1, Pallas kernels, local(): pl.pallas_call(functools.partial(branches, ep_size, tp_size, slice_rows,...  28.4 us
    pallas_call x1, Pallas kernels, local(): pl.pallas_call(mixer, out_shape=[jax.ShapeDtypeStruct((count, inner), bf1...  4.85 us

profile of v2, /device:TPU:0, one launch (start us, length us, event | category | flops | bytes accessed | tf_op | source)
XLA Modules:
  0.0 34.7 jit_solution(11200488451504198373)
XLA Ops:
  0.6 0.0 copy-start
  0.6 0.0 copy-start.1
  0.7 0.0 copy-start.2
  0.7 0.0 copy-start.3
  0.7 0.0 copy-start.4
  0.7 0.0 copy-start.5
  0.7 4.9 %shard_map.273 = (bf16[24,256]{1,0:T(8,128)(2,1)S(1)}, f32[24,4,64,128]{3,2,1,0:T(8,128)}, bf16[3,24,256]{2,1,0:T(8,128)(2,1)}, bf16[24,3,2,128]{3,2,1,0:T(2,128)(2,1)}) custom-call(bf16[24,1024]{1,0:T(8,128)(2,1)} %tokens.1, f32[1,1024]{1,0:T(1,128)} %bitcast.26, bf16[1024,256]{1,0:T(8,128)(2,1)} %gatew_hbm.1, bf16[1024,256]{1,0:T(8,128)(2,1)} %innerw_hbm.1, ...), custom_call_target="tpu_custom_call" | custom-call | tf_op jit(solution)/shard_map/pallas_call | solution.py:628
  5.6 0.0 copy-done
  5.6 0.0 copy-done.1
  5.6 0.0 copy-done.2
  5.6 0.0 copy-done.3
  5.6 0.0 copy-done.4
  5.6 0.0 copy-done.5
  5.6 28.4 %shard_map.274 = bf16[24,256]{1,0:T(8,128)(2,1)S(1)} custom-call(bf16[24,256]{1,0:T(8,128)(2,1)S(1)} %get-tuple-element.8.mrows, bf16[256,1024]{1,0:T(8,128)(2,1)S(1)} %copy-done, bf16[24,1024]{1,0:T(8,128)(2,1)S(1)} %copy-done.1, f32[1,1024]{1,0:T(1,128)S(1)} %bitcast.16, s32[2,24]{1,0:T(2,128)S(1)} %bitcast.17, f32[2,24]{1,0:T(2,128)S(1)} %bitcast.18, ...), custom_call_target="tpu_custom_call" | custom-call | tf_op jit(solution)/shard_map/pallas_call | solution.py:676
  34.1 0.6 %copy.31 = bf16[24,256]{1,0:T(8,128)(2,1)} copy(bf16[24,256]{1,0:T(8,128)(2,1)S(1)} %shard_map.274) | data formatting | bytes 24576
Async XLA Ops:
  0.6 4.9 %copy-start = (bf16[256,1024]{1,0:T(8,128)(2,1)S(1)}, bf16[256,1024]{1,0:T(8,128)(2,1)}, u32[]{:S(2)}) copy-start(bf16[256,1024]{1,0:T(8,128)(2,1)} %outw.1) | copy-start | bytes 1572868
  0.6 4.9 %copy-start.1 = (bf16[24,1024]{1,0:T(8,128)(2,1)S(1)}, bf16[24,1024]{1,0:T(8,128)(2,1)}, u32[]{:S(2)}) copy-start(bf16[24,1024]{1,0:T(8,128)(2,1)} %tokens.1) | copy-start | bytes 147460
  0.7 4.9 %copy-start.2 = (f32[1024]{0:T(1024)S(1)}, f32[1024]{0:T(1024)}, u32[]{:S(2)}) copy-start(f32[1024]{0:T(1024)} %param.42) | copy-start | bytes 12292
  0.7 4.9 %copy-start.3 = (s32[24,2]{0,1:T(2,128)S(1)}, s32[24,2]{0,1:T(2,128)}, u32[]{:S(2)}) copy-start(s32[24,2]{0,1:T(2,128)} %param.43) | copy-start | bytes 580
  0.7 4.9 %copy-start.4 = (f32[24,2]{0,1:T(2,128)S(1)}, f32[24,2]{0,1:T(2,128)}, u32[]{:S(2)}) copy-start(f32[24,2]{0,1:T(2,128)} %param.44) | copy-start | bytes 580
  0.7 4.9 %copy-start.5 = (f32[256]{0:T(256)S(1)}, f32[256]{0:T(256)}, u32[]{:S(2)}) copy-start(f32[256]{0:T(256)} %param.51) | copy-start | bytes 3076

commit v3 on v2

--- a/solution.py
+++ b/solution.py
@@ -13,7 +13,8 @@
 STATE_DIM = 128
 LANES = 128
 SEQ_STEP = 4
-ROW_ORDER = (7, 6, 5, 4, 3, 2, 1)
+RELAY_LAG = 8
+CHUNKS = ((0, 8),)
 
 eps = 1e-06
 
@@ -253,6 +254,7 @@
     weights_in,
     down_w,
     dense_w,
+    table_send,
     tables,
     part,
     parts,
@@ -261,10 +263,13 @@
     flat,
     pre,
     act,
+    hid,
+    shares,
     y_part,
     y_recv,
     z_send,
     z_recv,
+    near_sems,
     load_sems,
     part_sems,
     table_sems,
@@ -306,21 +311,32 @@
     def settle(ref, sem):
         pltpu.make_async_copy(ref, ref, sem).wait()
 
+    def tell(sem, to_e, to_t):
+        pl.semaphore_signal(
+            sem, inc=1, device_id=(to_e, to_t), device_id_type=pl.DeviceIdType.MESH
+        )
+
     barrier = pltpu.get_barrier_semaphore()
+    staged = ep_size == 8
+    line = me_e // 2
+    last = ep_size // 2 - 1
+
+    def tell_line(sem, distance, to_t):
+        pl.when(line >= distance)(lambda: tell(sem, me_e - 2 * distance, to_t))
+        pl.when(line + distance <= last)(lambda: tell(sem, me_e + 2 * distance, to_t))
+
+    def line_peers(distance):
+        below = jnp.where(line >= distance, 1, 0)
+        return below + jnp.where(line + distance <= last, 1, 0)
+
     for m in range(1, tp_size):
-        pl.semaphore_signal(
-            barrier,
-            inc=1,
-            device_id=(me_e, flip(me_t, m)),
-            device_id_type=pl.DeviceIdType.MESH,
-        )
-    for m in range(ep_size - 1, 0, -1):
-        pl.semaphore_signal(
-            barrier,
-            inc=1,
-            device_id=(flip(me_e, m), me_t),
-            device_id_type=pl.DeviceIdType.MESH,
-        )
+        tell(barrier, me_e, flip(me_t, m))
+    if staged:
+        tell(barrier, flip(me_e, 1), me_t)
+        tell_line(barrier, 1, me_t)
+    else:
+        for m in range(ep_size - 1, 0, -1):
+            tell(barrier, flip(me_e, m), partner)
 
     def dense_rows(ref, t):
         if slice_rows == hidden_width:
@@ -343,19 +359,22 @@
     table = jnp.zeros((ep_size, count), f32)
     for k in range(routes.shape[0]):
         table = table + jnp.where(expert_of == routes[k : k + 1, :], rweights[k : k + 1, :], 0.0)
-    tables[0] = jnp.concatenate([table, jnp.zeros((ep_size, LANES - count), f32)], axis=1)
+    table = jnp.concatenate([table, jnp.zeros((ep_size, LANES - count), f32)], axis=1)
+    for m in range(ep_size):
+        table_send[m] = table[m : m + 1]
+    tables[me_e] = table_send[me_e]
     scales[0] = scale[...]
 
-    pl.semaphore_wait(barrier, ep_size + tp_size - 2)
+    if staged:
+        pl.semaphore_wait(barrier, tp_size + line_peers(1))
+        tell_line(near_sems.at[0], 1, me_t)
+    else:
+        pl.semaphore_wait(barrier, ep_size + tp_size - 2)
     tp_order = [m for m in range(2, tp_size)] + [1]
     for m in tp_order:
         to = flip(me_t, m)
         remote(
             part.at[lax.rem(to, 2)], parts.at[m], part_sems.at[0], part_sems.at[1], me_e, to
-        )
-    for m in range(1, ep_size):
-        remote(
-            tables.at[0], tables.at[m], table_sems.at[0], table_sems.at[1], flip(me_e, m), me_t
         )
     for m in tp_order:
         to = flip(me_t, m)
@@ -370,6 +389,12 @@
                 to,
             )
 
+    if staged:
+        pl.semaphore_wait(near_sems.at[0], line_peers(1))
+        tell_line(near_sems.at[1], 1, me_t)
+        tell_line(near_sems.at[1], 2, me_t)
+        pl.semaphore_wait(near_sems.at[1], line_peers(1) + line_peers(2))
+        tell(near_sems.at[2], me_e, partner)
     own_rows = []
     for h in range(halves):
         at = pl.ds(pl.multiple_of(core * own_width + 2 * h * own_width, own_width), own_width)
@@ -379,55 +404,94 @@
         for m in range(1, tp_size):
             own_rows[h] = own_rows[h] + parts[m, h].astype(f32)
         residual[h] = own_rows[h]
-        rows[core, 0, h] = own_rows[h].astype(bf16)
-
-    row_copies = {}
-    for m in ROW_ORDER if ep_size == 8 else range(1, ep_size):
-        row_copies[m] = remote(
-            rows.at[core, 0],
-            rows.at[core, m],
+        rows[core, me_e, h] = own_rows[h].astype(bf16)
+
+    if staged:
+        pl.semaphore_wait(near_sems.at[2], 1)
+    for m in range(ep_size - 1, 0, -1):
+        remote(
+            rows.at[core, me_e],
+            rows.at[core, me_e],
             row_send.at[0],
-            row_sems.at[m],
+            row_sems.at[me_e],
             flip(me_e, m),
-            me_t,
-        )
-
-    relay_copies = {}
-
-    def relay(m):
-        if m:
-            row_copies[m].wait_recv()
-        relay_copies[m] = remote(
-            rows.at[core, m],
-            rows.at[core, m],
-            relay_send.at[0],
-            relay_sems.at[m],
-            me_e,
             partner,
         )
-
-    def normalize(m, at):
-        relay_copies[m].wait_recv()
-        pieces = [rows[q % 2, m, q // 2].astype(f32) for q in range(tp_size)]
-        squares = pieces[0] * pieces[0]
-        for q in range(1, tp_size):
-            squares = squares + pieces[q] * pieces[q]
-        scale_of = lax.rsqrt(jnp.sum(squares, axis=-1, keepdims=True) * (1.0 / width) + eps)
-        for q in range(tp_size):
-            lanes = slice(q * own_width, (q + 1) * own_width)
-            flat[at * count : (at + 1) * count, lanes] = pieces[q] * scale_of * gain[:, lanes]
-
-    unit = 64 if expert_hidden % 64 == 0 else expert_hidden
+    for m in range(1, ep_size):
+        remote(
+            table_send.at[flip(me_e, m)],
+            tables.at[me_e],
+            table_sems.at[0],
+            table_sems.at[1],
+            flip(me_e, m),
+            partner,
+        )
+
+    def block_of(chunk, place):
+        start, length = chunk
+        return start + flip(lax.rem(me_e, length), place)
+
+    def is_home(chunk):
+        start, length = chunk
+        return me_e // length == start // length
+
+    def relay(chunk, place):
+        m = block_of(chunk, place)
+
+        def pass_on(half):
+            remote(
+                rows.at[half, m],
+                rows.at[half, m],
+                relay_send.at[0],
+                relay_sems.at[m],
+                me_e,
+                partner,
+            )
+
+        def forward():
+            settle(rows.at[1 - core, m], row_sems.at[m])
+            pass_on(1 - core)
+
+        if place:
+            forward()
+        else:
+            home = is_home(chunk)
+            pl.when(home)(lambda: pass_on(core))
+            pl.when(jnp.logical_not(home))(forward)
+
+    def normalize(chunk, places):
+        blocks = [(at, block_of(chunk, at)) for at in places]
+        for at, m in blocks:
+            settle(rows.at[core, m], relay_sems.at[m])
+        for at, m in blocks:
+            pieces = [rows[q % 2, m, q // 2].astype(f32) for q in range(tp_size)]
+            squares = pieces[0] * pieces[0]
+            for q in range(1, tp_size):
+                squares = squares + pieces[q] * pieces[q]
+            scale_of = lax.rsqrt(jnp.sum(squares, axis=-1, keepdims=True) * (1.0 / width) + eps)
+            for q in range(tp_size):
+                lanes = slice(q * own_width, (q + 1) * own_width)
+                flat[at * count : (at + 1) * count, lanes] = pieces[q] * scale_of * gain[:, lanes]
+
+    unit = LANES
     if slice_rows == hidden_width:
         units = lax.broadcasted_iota(jnp.int32, (slice_rows, 1), 0)
         share = hidden_width // tp_size
         kept = (units // share == me_t).astype(f32)
 
+    def weigh(m):
+        row = tables[m][:, :count]
+        diagonal = lax.broadcasted_iota(jnp.int32, (count, count), 0) == lax.broadcasted_iota(
+            jnp.int32, (count, count), 1
+        )
+        weight = jnp.sum(jnp.where(diagonal, row, 0.0), axis=1, keepdims=True)
+        shares[m] = jnp.broadcast_to(weight, (count, own_width))
+
     def place_weights():
         settle(weights_in.at[pl.ds(0, 2 * expert_hidden)], load_sems.at[0])
         settle(down_w, load_sems.at[1])
         settle(dense_w.at[0], load_sems.at[2])
-        settle(tables.at[pl.ds(1, ep_size - 1)], table_sems.at[1])
+        settle(tables.at[pl.ds(0, ep_size - 1)], table_sems.at[1])
         settle(scales.at[pl.ds(1, tp_size - 1)], scale_sems.at[1])
         settle(dense_w.at[pl.ds(1, tp_size - 1)], dense_sems.at[1])
         for k in range(2):
@@ -435,129 +499,107 @@
             for m in range(tp_size):
                 lanes = pl.ds(pl.multiple_of(flip(me_t, m) * own_width, own_width), own_width)
                 weights_in[at, lanes] = dense_w[m, k]
+        for m in range(ep_size):
+            weigh(m)
 
     def activate(chunk):
-        live = len(chunk) * count
+        live = chunk[1] * count
         lanes = slice(0, live)
         x = flat[:live, :].astype(bf16)
         pre[:, lanes] = dot_rows(weights_in[...], x)
         for n in range(0, expert_hidden, unit):
-            gate_act = pre[n : n + unit, lanes]
-            up_act = pre[expert_hidden + n : expert_hidden + n + unit, lanes]
-            act[n : n + unit, lanes] = (silu(gate_act) * up_act).astype(bf16)
+            end = min(n + unit, expert_hidden)
+            gate_act = pre[n:end, lanes]
+            up_act = pre[expert_hidden + n : expert_hidden + end, lanes]
+            act[lanes, n:end] = (silu(gate_act) * up_act).T.astype(bf16)
         gate_act = pre[dense_at[0] : dense_at[0] + slice_rows, lanes]
         up_act = pre[dense_at[1] : dense_at[1] + slice_rows, lanes]
         hidden = silu(gate_act) * up_act
         if slice_rows == hidden_width:
             hidden = hidden * kept
-        act[expert_hidden : expert_hidden + slice_rows, lanes] = hidden.astype(bf16)
-
-    def weigh(m):
-        held = tables[m]
-        mine = lax.broadcasted_iota(jnp.int32, held.shape, 0) == me_e
-        row = jnp.sum(jnp.where(mine, held, 0.0), axis=0, keepdims=True)[:, :count]
-        diagonal = lax.broadcasted_iota(jnp.int32, (count, count), 0) == lax.broadcasted_iota(
-            jnp.int32, (count, count), 1
-        )
-        return jnp.sum(jnp.where(diagonal, row, 0.0), axis=1, keepdims=True)
+        hid[:, lanes] = hidden.astype(bf16)
 
     contract_rows = (((0,), (0,)), ((), ()))
 
     def project(chunk, first):
-        live = len(chunk) * count
-        weights = [weigh(m) for m in chunk]
-        acts = act[:expert_hidden, :live]
-        hidden = act[expert_hidden : expert_hidden + slice_rows, :live]
-        sent = None
+        live = chunk[1] * count
+        weights = [shares[block_of(chunk, g)] for g in range(chunk[1])]
+        acts = act[:live, :]
+        hidden = hid[:, :live]
         for mine in range(2):
-            whose = core if mine else 1 - core
+            whose = 1 - core if mine else core
             for h in range(halves):
                 t = 2 * h + whose
                 lanes = pl.ds(pl.multiple_of(t * own_width, own_width), own_width)
                 slot = flipped(me_t, t)
-                routed = lax.dot_general(
-                    acts, down_w[:, lanes], contract_rows, preferred_element_type=f32
-                )
+                routed = dot(acts, down_w[:, lanes])
                 dense = lax.dot_general(
                     hidden, dense_w[slot, 2], contract_rows, preferred_element_type=f32
                 )
-                for g in range(len(chunk)):
+                for g in range(chunk[1]):
                     at = slice(g * count, (g + 1) * count)
                     y = routed[at] * weights[g] + dense[at] * scales[slot]
                     y_part[mine, h, first + g] = y.astype(bf16)
-            if not mine:
-                at = pl.ds(first, len(chunk))
-                sent = remote(
-                    y_part.at[0, :, at],
-                    y_recv.at[:, at],
-                    y_sems.at[0, len(y_copies)],
-                    y_sems.at[1, len(y_copies)],
-                    me_e,
-                    partner,
-                )
-        y_copies.append(sent)
-
+                if not mine:
+                    at = pl.ds(first, chunk[1])
+                    y_copies.append(
+                        remote(
+                            y_part.at[0, h, at],
+                            y_recv.at[h, at],
+                            y_sems.at[0, len(y_copies)],
+                            y_sems.at[1, len(y_copies)],
+                            me_e,
+                            partner,
+                        )
+                    )
     def give_back(chunk, first, sent):
-        sent.wait_recv()
-        kept_sum = None
-        for g in reversed(range(len(chunk))):
-            m = chunk[g]
-            for o in range(halves - 1, -1, -1):
-                to_side = flip(side, o)
+        for to_side in range(halves):
+            sent[to_side].wait_recv()
+            for g in range(chunk[1] - 1, -1, -1):
+                m = block_of(chunk, g)
+                at = to_side * ep_size + first + g
                 summed = y_part[1, to_side, first + g].astype(f32)
                 summed = summed + y_recv[to_side, first + g].astype(f32)
-                if m == 0 and o == 0:
-                    kept_sum = summed
-                    continue
-                z_send[o * ep_size + m] = summed.astype(bf16)
+
+                z_send[at] = summed.astype(bf16)
                 remote(
-                    z_send.at[o * ep_size + m],
-                    z_recv.at[o * ep_size + m],
+                    z_send.at[at],
+                    z_recv.at[side * ep_size + me_e],
                     z_sems.at[0],
                     z_sems.at[1],
-                    flip(me_e, m),
-                    2 * to_side + core,
+                    m,
+                    2 * to_side + 1 - core,
                 )
-        return kept_sum
 
     y_copies = []
-    firsts = [sum(len(c) for c in chunks[:k]) for k in range(len(chunks))]
-    for m in chunks[0]:
-        relay(m)
-    for at, m in enumerate(chunks[0]):
-        normalize(m, at)
-    place_weights()
-    activate(chunks[0])
-    final = None
     for k, chunk in enumerate(chunks):
-        after = chunks[k + 1] if k + 1 < len(chunks) else []
-        for m in after:
-            relay(m)
-        project(chunk, firsts[k])
-        for at, m in enumerate(after):
-            normalize(m, at)
-        if after:
-            activate(after)
-        kept_sum = give_back(chunk, firsts[k], y_copies[k])
-        if kept_sum is not None:
-            final = residual[side] + kept_sum
-
-    settle(z_recv.at[pl.ds(1, halves * ep_size - 1)], z_sems.at[1])
-    for o in range(halves):
-        for m in range(ep_size):
-            if m or o:
-                final = final + z_recv[o * ep_size + m].astype(f32)
+        late = max(chunk[1] - RELAY_LAG, 0)
+        for place in range(chunk[1]):
+            relay(chunk, place)
+            if place >= RELAY_LAG:
+                normalize(chunk, [place - RELAY_LAG])
+        if k == 0:
+            place_weights()
+        normalize(chunk, range(late, chunk[1]))
+        activate(chunk)
+        project(chunk, chunk[0])
+        give_back(chunk, chunk[0], y_copies[halves * k :])
+
+    settle(z_recv, z_sems.at[1])
+    final = residual[side]
+    for m in range(halves * ep_size):
+        final = final + z_recv[m].astype(f32)
     out[...] = final.astype(bf16)
 
     settle(parts.at[pl.ds(1, tp_size - 1)], part_sems.at[0])
-    settle(tables.at[pl.ds(1, ep_size - 1)], table_sems.at[0])
+    settle(tables.at[pl.ds(0, ep_size - 1)], table_sems.at[0])
     settle(scales.at[pl.ds(1, tp_size - 1)], scale_sems.at[0])
     settle(dense_w.at[pl.ds(1, tp_size - 1)], dense_sems.at[0])
     settle(rows.at[0, pl.ds(1, ep_size - 1)], row_send.at[0])
     settle(rows.at[0], relay_send.at[0])
     for copy in y_copies:
         copy.wait_send()
-    settle(z_send.at[pl.ds(1, halves * ep_size - 1)], z_sems.at[0])
+    settle(z_send, z_sems.at[0])
 
 
 def local(
@@ -654,9 +696,8 @@
     if hidden_width % (8 * tp_size):
         slice_rows = hidden_width
     halves = tp_size // 2
-    chunk_len = min(ep_size, 4 if ep_size <= 8 else 8)
-    chunks = [list(range(k, k + chunk_len)) for k in range(0, ep_size, chunk_len)]
-    live = chunk_len * count
+    chunks = CHUNKS if ep_size == 8 else [(k, 8) for k in range(0, ep_size, 8)]
+    live = max(length for _, length in chunks) * count
     wide = 2 * (expert_hidden + padded(slice_rows))
     branch_args = [
         mixer_rows,
@@ -683,18 +724,22 @@
             vmem((wide, width), bf16),
             vmem(expert_down.shape[1:], bf16),
             vmem((tp_size, 3, slice_rows, own_width), bf16),
-            vmem((ep_size, ep_size, LANES), f32),
+            vmem((ep_size, 1, LANES), f32),
+            vmem((ep_size, 1, LANES), f32),
             vmem((2, halves, count, own_width), bf16),
             vmem((tp_size, halves, count, own_width), bf16),
             vmem((halves, count, own_width), f32),
             vmem((2, ep_size, halves, count, own_width), bf16),
             vmem((live, width), f32),
             vmem((wide, live), f32),
-            vmem((expert_hidden + padded(slice_rows), live), bf16),
+            vmem((live, expert_hidden), bf16),
+            vmem((slice_rows, live), bf16),
+            vmem((ep_size, count, own_width), f32),
             vmem((2, halves, ep_size, count, own_width), bf16),
             vmem((halves, ep_size, count, own_width), bf16),
             vmem((halves * ep_size, count, own_width), bf16),
             vmem((halves * ep_size, count, own_width), bf16),
+            pltpu.SemaphoreType.REGULAR((3,)),
             dma((3,)),
             dma((2,)),
             dma((2,)),
@@ -704,7 +749,7 @@
             dma((ep_size,)),
             dma((1,)),
             dma((ep_size,)),
-            dma((2, len(chunks))),
+            dma((2, halves * len(chunks))),
             dma((2,)),
         ],
         compiler_params=pltpu.CompilerParams(

time: 34.8 us -> 30.1 us (0.86)
  the two profiles are of different devices: /device:TPU:0 before, /device:TPU:3 now
where the time goes in v3:
time: 30.1 us; the launch traced here: 30 us
  Pallas kernels  28.6 us (95%)
  between operations  0.75 us (2%)
  local copies, waits for them, and re-layouts  0.63 us (2%)
    pallas_call x1, Pallas kernels, local(): pl.pallas_call(functools.partial(branches, ep_size, tp_size, slice_rows,...  23.7 us
    pallas_call x1, Pallas kernels, local(): pl.pallas_call(mixer, out_shape=[jax.ShapeDtypeStruct((count, inner), bf1...  4.86 us
    unnamed x13, local copies, waits for them, and re-layouts  0.63 us

profile of v3, /device:TPU:3, one launch (start us, length us, event | category | flops | bytes accessed | tf_op | source)
XLA Modules:
  0.0 30.0 jit_solution(8465608588172660956)
XLA Ops:
  0.6 0.0 copy-start
  0.6 0.0 copy-start.1
  0.7 0.0 copy-start.2
  0.7 0.0 copy-start.3
  0.7 0.0 copy-start.4
  0.7 0.0 copy-start.5
  0.7 4.9 %shard_map.273 = (bf16[24,256]{1,0:T(8,128)(2,1)S(1)}, f32[24,4,64,128]{3,2,1,0:T(8,128)}, bf16[3,24,256]{2,1,0:T(8,128)(2,1)}, bf16[24,3,2,128]{3,2,1,0:T(2,128)(2,1)}) custom-call(bf16[24,1024]{1,0:T(8,128)(2,1)} %tokens.1, f32[1,1024]{1,0:T(1,128)} %bitcast.26, bf16[1024,256]{1,0:T(8,128)(2,1)} %gatew_hbm.1, bf16[1024,256]{1,0:T(8,128)(2,1)} %innerw_hbm.1, ...), custom_call_target="tpu_custom_call" | custom-call | tf_op jit(solution)/shard_map/pallas_call | solution.py:670
  5.6 0.0 copy-done
  5.6 0.0 copy-done.1
  5.6 0.0 copy-done.2
  5.6 0.0 copy-done.3
  5.6 0.0 copy-done.4
  5.6 0.0 copy-done.5
  5.6 23.7 %shard_map.274 = bf16[24,256]{1,0:T(8,128)(2,1)S(1)} custom-call(bf16[24,256]{1,0:T(8,128)(2,1)S(1)} %get-tuple-element.8.mrows, bf16[256,1024]{1,0:T(8,128)(2,1)S(1)} %copy-done, bf16[24,1024]{1,0:T(8,128)(2,1)S(1)} %copy-done.1, f32[1,1024]{1,0:T(1,128)S(1)} %bitcast.16, s32[2,24]{1,0:T(2,128)S(1)} %bitcast.17, f32[2,24]{1,0:T(2,128)S(1)} %bitcast.18, ...), custom_call_target="tpu_custom_call" | custom-call | tf_op jit(solution)/shard_map/pallas_call | solution.py:717
  29.4 0.6 %copy.31 = bf16[24,256]{1,0:T(8,128)(2,1)} copy(bf16[24,256]{1,0:T(8,128)(2,1)S(1)} %shard_map.274) | data formatting | bytes 24576
Async XLA Ops:
  0.6 4.9 %copy-start = (bf16[256,1024]{1,0:T(8,128)(2,1)S(1)}, bf16[256,1024]{1,0:T(8,128)(2,1)}, u32[]{:S(2)}) copy-start(bf16[256,1024]{1,0:T(8,128)(2,1)} %outw.1) | copy-start | bytes 1572868
  0.6 4.9 %copy-start.1 = (bf16[24,1024]{1,0:T(8,128)(2,1)S(1)}, bf16[24,1024]{1,0:T(8,128)(2,1)}, u32[]{:S(2)}) copy-start(bf16[24,1024]{1,0:T(8,128)(2,1)} %tokens.1) | copy-start | bytes 147460
  0.7 4.9 %copy-start.2 = (f32[1024]{0:T(1024)S(1)}, f32[1024]{0:T(1024)}, u32[]{:S(2)}) copy-start(f32[1024]{0:T(1024)} %param.42) | copy-start | bytes 12292
  0.7 4.9 %copy-start.3 = (s32[24,2]{0,1:T(2,128)S(1)}, s32[24,2]{0,1:T(2,128)}, u32[]{:S(2)}) copy-start(s32[24,2]{0,1:T(2,128)} %param.43) | copy-start | bytes 580
  0.7 4.9 %copy-start.4 = (f32[24,2]{0,1:T(2,128)S(1)}, f32[24,2]{0,1:T(2,128)}, u32[]{:S(2)}) copy-start(f32[24,2]{0,1:T(2,128)} %param.44) | copy-start | bytes 580
  0.7 4.9 %copy-start.5 = (f32[256]{0:T(256)S(1)}, f32[256]{0:T(256)}, u32[]{:S(2)}) copy-start(f32[256]{0:T(256)} %param.51) | copy-start | bytes 3076

commit v4 on v3

--- a/solution.py
+++ b/solution.py
@@ -12,7 +12,8 @@
 HEAD_DIM = 64
 STATE_DIM = 128
 LANES = 128
-SEQ_STEP = 4
+SEQ_STEP = 6
+DEST_ORDER = (0, 1, 7, 6, 5, 4, 3, 2)
 RELAY_LAG = 8
 CHUNKS = ((0, 8),)
 
@@ -355,14 +356,6 @@
     for q in range(tp_size):
         piece = dot(mixer_rows, outw[:, q * own_width : (q + 1) * own_width])
         part[q % 2, q // 2] = piece.astype(bf16)
-    expert_of = lax.broadcasted_iota(jnp.int32, (ep_size, count), 0)
-    table = jnp.zeros((ep_size, count), f32)
-    for k in range(routes.shape[0]):
-        table = table + jnp.where(expert_of == routes[k : k + 1, :], rweights[k : k + 1, :], 0.0)
-    table = jnp.concatenate([table, jnp.zeros((ep_size, LANES - count), f32)], axis=1)
-    for m in range(ep_size):
-        table_send[m] = table[m : m + 1]
-    tables[me_e] = table_send[me_e]
     scales[0] = scale[...]
 
     if staged:
@@ -389,6 +382,14 @@
                 to,
             )
 
+    expert_of = lax.broadcasted_iota(jnp.int32, (ep_size, count), 0)
+    table = jnp.zeros((ep_size, count), f32)
+    for k in range(routes.shape[0]):
+        table = table + jnp.where(expert_of == routes[k : k + 1, :], rweights[k : k + 1, :], 0.0)
+    table = jnp.concatenate([table, jnp.zeros((ep_size, LANES - count), f32)], axis=1)
+    for m in range(ep_size):
+        table_send[m] = table[m : m + 1]
+    tables[me_e] = table_send[me_e]
     if staged:
         pl.semaphore_wait(near_sems.at[0], line_peers(1))
         tell_line(near_sems.at[1], 1, me_t)
@@ -555,12 +556,16 @@
     def give_back(chunk, first, sent):
         for to_side in range(halves):
             sent[to_side].wait_recv()
-            for g in range(chunk[1] - 1, -1, -1):
-                m = block_of(chunk, g)
-                at = to_side * ep_size + first + g
-                summed = y_part[1, to_side, first + g].astype(f32)
-                summed = summed + y_recv[to_side, first + g].astype(f32)
-
+            for n in range(chunk[1]):
+                if ep_size == 8:
+                    m = DEST_ORDER[n]
+                    place = flip(me_e, m)
+                else:
+                    place = first + chunk[1] - 1 - n
+                    m = block_of(chunk, chunk[1] - 1 - n)
+                at = to_side * ep_size + place
+                summed = y_part[1, to_side, place].astype(f32)
+                summed = summed + y_recv[to_side, place].astype(f32)
                 z_send[at] = summed.astype(bf16)
                 remote(
                     z_send.at[at],

time: 30.1 us -> 29.5 us (0.980)
  the two profiles are of different devices: /device:TPU:3 before, /device:TPU:0 now
where the time goes in v4:
time: 29.5 us; the launch traced here: 29.3 us
  Pallas kernels  27.9 us (95%)
  between operations  0.75 us (3%)
  local copies, waits for them, and re-layouts  0.63 us (2%)
    pallas_call x1, Pallas kernels, local(): pl.pallas_call(functools.partial(branches, ep_size, tp_size, slice_rows,...  23.1 us
    pallas_call x1, Pallas kernels, local(): pl.pallas_call(mixer, out_shape=[jax.ShapeDtypeStruct((count, inner), bf1...  4.73 us
    unnamed x13, local copies, waits for them, and re-layouts  0.63 us

profile of v4, /device:TPU:0, one launch (start us, length us, event | category | flops | bytes accessed | tf_op | source)
XLA Modules:
  0.0 29.3 jit_solution(1594866738731972100)
XLA Ops:
  0.6 0.0 copy-start
  0.6 0.0 copy-start.1
  0.7 0.0 copy-start.2
  0.7 0.0 copy-start.3
  0.7 0.0 copy-start.4
  0.7 0.0 copy-start.5
  0.7 4.7 %shard_map.273 = (bf16[24,256]{1,0:T(8,128)(2,1)S(1)}, f32[24,4,64,128]{3,2,1,0:T(8,128)}, bf16[3,24,256]{2,1,0:T(8,128)(2,1)}, bf16[24,3,2,128]{3,2,1,0:T(2,128)(2,1)}) custom-call(bf16[24,1024]{1,0:T(8,128)(2,1)} %tokens.1, f32[1,1024]{1,0:T(1,128)} %bitcast.26, bf16[1024,256]{1,0:T(8,128)(2,1)} %gatew_hbm.1, bf16[1024,256]{1,0:T(8,128)(2,1)} %innerw_hbm.1, ...), custom_call_target="tpu_custom_call" | custom-call | tf_op jit(solution)/shard_map/pallas_call | solution.py:675
  5.4 0.0 copy-done
  5.4 0.0 copy-done.1
  5.5 0.0 copy-done.2
  5.5 0.0 copy-done.3
  5.5 0.0 copy-done.4
  5.5 0.0 copy-done.5
  5.5 23.1 %shard_map.274 = bf16[24,256]{1,0:T(8,128)(2,1)S(1)} custom-call(bf16[24,256]{1,0:T(8,128)(2,1)S(1)} %get-tuple-element.8.mrows, bf16[256,1024]{1,0:T(8,128)(2,1)S(1)} %copy-done, bf16[24,1024]{1,0:T(8,128)(2,1)S(1)} %copy-done.1, f32[1,1024]{1,0:T(1,128)S(1)} %bitcast.16, s32[2,24]{1,0:T(2,128)S(1)} %bitcast.17, f32[2,24]{1,0:T(2,128)S(1)} %bitcast.18, ...), custom_call_target="tpu_custom_call" | custom-call | tf_op jit(solution)/shard_map/pallas_call | solution.py:722
  28.7 0.6 %copy.31 = bf16[24,256]{1,0:T(8,128)(2,1)} copy(bf16[24,256]{1,0:T(8,128)(2,1)S(1)} %shard_map.274) | data formatting | bytes 24576
Async XLA Ops:
  0.6 4.8 %copy-start = (bf16[256,1024]{1,0:T(8,128)(2,1)S(1)}, bf16[256,1024]{1,0:T(8,128)(2,1)}, u32[]{:S(2)}) copy-start(bf16[256,1024]{1,0:T(8,128)(2,1)} %outw.1) | copy-start | bytes 1572868
  0.6 4.8 %copy-start.1 = (bf16[24,1024]{1,0:T(8,128)(2,1)S(1)}, bf16[24,1024]{1,0:T(8,128)(2,1)}, u32[]{:S(2)}) copy-start(bf16[24,1024]{1,0:T(8,128)(2,1)} %tokens.1) | copy-start | bytes 147460
  0.7 4.8 %copy-start.2 = (f32[1024]{0:T(1024)S(1)}, f32[1024]{0:T(1024)}, u32[]{:S(2)}) copy-start(f32[1024]{0:T(1024)} %param.42) | copy-start | bytes 12292
  0.7 4.8 %copy-start.3 = (s32[24,2]{0,1:T(2,128)S(1)}, s32[24,2]{0,1:T(2,128)}, u32[]{:S(2)}) copy-start(s32[24,2]{0,1:T(2,128)} %param.43) | copy-start | bytes 580
  0.7 4.8 %copy-start.4 = (f32[24,2]{0,1:T(2,128)S(1)}, f32[24,2]{0,1:T(2,128)}, u32[]{:S(2)}) copy-start(f32[24,2]{0,1:T(2,128)} %param.44) | copy-start | bytes 580
  0.7 4.8 %copy-start.5 = (f32[256]{0:T(256)S(1)}, f32[256]{0:T(256)}, u32[]{:S(2)}) copy-start(f32[256]{0:T(256)} %param.51) | copy-start | bytes 3076

commit v5 on v4

--- a/solution.py
+++ b/solution.py
@@ -14,7 +14,6 @@
 LANES = 128
 SEQ_STEP = 6
 DEST_ORDER = (0, 1, 7, 6, 5, 4, 3, 2)
-RELAY_LAG = 8
 CHUNKS = ((0, 8),)
 
 eps = 1e-06
@@ -102,7 +101,8 @@
     loads = []
     for i, (src, dst) in enumerate(small):
         copy = pltpu.make_async_copy(src, dst, sems.at[i])
-        copy.start()
+        if i < 11:
+            copy.start()
         loads.append(copy)
 
     def state_load(i):
@@ -118,16 +118,17 @@
     loads[1].wait()
     for i in range(steps):
         state_load(i).start()
+    for copy in loads[11:]:
+        copy.start()
     value = tokens[...].astype(f32)
     squares = jnp.mean(value * value, axis=-1, keepdims=True)
     normed = (value * lax.rsqrt(squares + eps) * mgain[...]).astype(bf16)
-    for i in range(2, 14):
+    for i in range(2, 11):
         loads[i].wait()
     inner_pre = dot(normed, innerw[...]).astype(bf16)
     pre_u = dot(normed, statew[0])
     pre_c = dot(normed, statew[1])
     step_raw = dot_rows(normed, stepw[...])
-    gate_pre = dot(normed, gatew[...])
 
     iwin[taps - 1] = inner_pre
     conv = inner_pre.astype(f32) * ikern[taps - 1 : taps, :]
@@ -196,6 +197,9 @@
                     )
         state_store(i).start()
 
+    for i in range(11, 14):
+        loads[i].wait()
+    gate_pre = dot(normed, gatew[...])
     read = mixed[...].T
     even = lax.rem(lax.broadcasted_iota(jnp.int32, (count, inner), 0), 2) == 0
     read = jnp.where(even, read[:count], read[count:])
@@ -444,7 +448,7 @@
                 rows.at[half, m],
                 rows.at[half, m],
                 relay_send.at[0],
-                relay_sems.at[m],
+                relay_sems.at[chunk[0] // chunk[1]],
                 me_e,
                 partner,
             )
@@ -462,8 +466,8 @@
 
     def normalize(chunk, places):
         blocks = [(at, block_of(chunk, at)) for at in places]
-        for at, m in blocks:
-            settle(rows.at[core, m], relay_sems.at[m])
+        sem = relay_sems.at[chunk[0] // chunk[1]]
+        settle(rows.at[0, pl.ds(chunk[0], chunk[1])], sem)
         for at, m in blocks:
             pieces = [rows[q % 2, m, q // 2].astype(f32) for q in range(tp_size)]
             squares = pieces[0] * pieces[0]
@@ -578,14 +582,11 @@
 
     y_copies = []
     for k, chunk in enumerate(chunks):
-        late = max(chunk[1] - RELAY_LAG, 0)
         for place in range(chunk[1]):
             relay(chunk, place)
-            if place >= RELAY_LAG:
-                normalize(chunk, [place - RELAY_LAG])
         if k == 0:
             place_weights()
-        normalize(chunk, range(late, chunk[1]))
+        normalize(chunk, range(chunk[1]))
         activate(chunk)
         project(chunk, chunk[0])
         give_back(chunk, chunk[0], y_copies[halves * k :])
@@ -753,7 +754,7 @@
             dma((1,)),
             dma((ep_size,)),
             dma((1,)),
-            dma((ep_size,)),
+            dma((len(chunks),)),
             dma((2, halves * len(chunks))),
             dma((2,)),
         ],

time: 29.5 us -> 29.2 us (0.990)
  no operation moved by 1% of the time
where the time goes in v5:
time: 29.2 us; the launch traced here: 29 us
  Pallas kernels  27.7 us (95%)
  between operations  0.75 us (3%)
  local copies, waits for them, and re-layouts  0.63 us (2%)
    pallas_call x1, Pallas kernels, local(): pl.pallas_call(functools.partial(branches, ep_size, tp_size, slice_rows,...  23.1 us
    pallas_call x1, Pallas kernels, local(): pl.pallas_call(mixer, out_shape=[jax.ShapeDtypeStruct((count, inner), bf1...  4.57 us
    unnamed x13, local copies, waits for them, and re-layouts  0.63 us

profile of v5, /device:TPU:0, one launch (start us, length us, event | category | flops | bytes accessed | tf_op | source)
XLA Modules:
  0.0 29.0 jit_solution(13049671227854016089)
XLA Ops:
  0.6 0.0 copy-start
  0.6 0.0 copy-start.1
  0.7 0.0 copy-start.2
  0.7 0.0 copy-start.3
  0.7 0.0 copy-start.4
  0.7 0.0 copy-start.5
  0.7 4.6 %shard_map.273 = (bf16[24,256]{1,0:T(8,128)(2,1)S(1)}, f32[24,4,64,128]{3,2,1,0:T(8,128)}, bf16[3,24,256]{2,1,0:T(8,128)(2,1)}, bf16[24,3,2,128]{3,2,1,0:T(2,128)(2,1)}) custom-call(bf16[24,1024]{1,0:T(8,128)(2,1)} %tokens.1, f32[1,1024]{1,0:T(1,128)} %bitcast.26, bf16[1024,256]{1,0:T(8,128)(2,1)} %gatew_hbm.1, bf16[1024,256]{1,0:T(8,128)(2,1)} %innerw_hbm.1, ...), custom_call_target="tpu_custom_call" | custom-call | tf_op jit(solution)/shard_map/pallas_call | solution.py:676
  5.3 0.0 copy-done
  5.3 0.0 copy-done.1
  5.3 0.0 copy-done.2
  5.3 0.0 copy-done.3
  5.3 0.0 copy-done.4
  5.3 0.0 copy-done.5
  5.3 23.1 %shard_map.274 = bf16[24,256]{1,0:T(8,128)(2,1)S(1)} custom-call(bf16[24,256]{1,0:T(8,128)(2,1)S(1)} %get-tuple-element.8.mrows, bf16[256,1024]{1,0:T(8,128)(2,1)S(1)} %copy-done, bf16[24,1024]{1,0:T(8,128)(2,1)S(1)} %copy-done.1, f32[1,1024]{1,0:T(1,128)S(1)} %bitcast.16, s32[2,24]{1,0:T(2,128)S(1)} %bitcast.17, f32[2,24]{1,0:T(2,128)S(1)} %bitcast.18, ...), custom_call_target="tpu_custom_call" | custom-call | tf_op jit(solution)/shard_map/pallas_call | solution.py:723
  28.4 0.6 %copy.31 = bf16[24,256]{1,0:T(8,128)(2,1)} copy(bf16[24,256]{1,0:T(8,128)(2,1)S(1)} %shard_map.274) | data formatting | bytes 24576
Async XLA Ops:
  0.6 4.6 %copy-start = (bf16[256,1024]{1,0:T(8,128)(2,1)S(1)}, bf16[256,1024]{1,0:T(8,128)(2,1)}, u32[]{:S(2)}) copy-start(bf16[256,1024]{1,0:T(8,128)(2,1)} %outw.1) | copy-start | bytes 1572868
  0.6 4.6 %copy-start.1 = (bf16[24,1024]{1,0:T(8,128)(2,1)S(1)}, bf16[24,1024]{1,0:T(8,128)(2,1)}, u32[]{:S(2)}) copy-start(bf16[24,1024]{1,0:T(8,128)(2,1)} %tokens.1) | copy-start | bytes 147460
  0.7 4.6 %copy-start.2 = (f32[1024]{0:T(1024)S(1)}, f32[1024]{0:T(1024)}, u32[]{:S(2)}) copy-start(f32[1024]{0:T(1024)} %param.42) | copy-start | bytes 12292
  0.7 4.6 %copy-start.3 = (s32[24,2]{0,1:T(2,128)S(1)}, s32[24,2]{0,1:T(2,128)}, u32[]{:S(2)}) copy-start(s32[24,2]{0,1:T(2,128)} %param.43) | copy-start | bytes 580
  0.7 4.6 %copy-start.4 = (f32[24,2]{0,1:T(2,128)S(1)}, f32[24,2]{0,1:T(2,128)}, u32[]{:S(2)}) copy-start(f32[24,2]{0,1:T(2,128)} %param.44) | copy-start | bytes 580
  0.7 4.6 %copy-start.5 = (f32[256]{0:T(256)S(1)}, f32[256]{0:T(256)}, u32[]{:S(2)}) copy-start(f32[256]{0:T(256)} %param.51) | copy-start | bytes 3076
